TPU v7x, 32 devices: a whole 2x2x4 slice. The times are simulated.
32 devices in a mesh: sp: 16 (over z, y, x), tp: 2 (over core).
Axes of the slice: x: 2, y: 2, z: 4, core: 2. Of those that a mesh axis runs over, the one named last changes fastest.
Arguments:
- moe_input: bfloat16 [2048, 2048], P('sp'), may hold values from -6 to 6
- out_grad: bfloat16 [2048, 2048], P('sp'), may hold values from -8 to 8
- route_ids: int32 [2048, 2], P('sp'), may hold values from 0 to 7, all different within a row; in each aligned block of 128 rows (0 to 127, 128 to 255, ...) at most 48 rows name the same one
- route_weights: float32 [2048, 2], P('sp'), may hold values from 0.1 to 0.9
- gate_w: bfloat16 [16, 2048, 1792], P('sp', None, 'tp'), may hold values from -0.125 to 0.125
- up_w: bfloat16 [16, 2048, 1792], P('sp', None, 'tp'), may hold values from -0.125 to 0.125
- down_w: bfloat16 [16, 1792, 2048], P('sp', 'tp'), may hold values from -0.09375 to 0.09375
- mixer_out: bfloat16 [2048, 1024], P('sp', 'tp'), may hold values from -6 to 6
- out_weight: bfloat16 [1024, 2048], P('tp'), may hold values from -0.1875 to 0.1875
- queries: bfloat16 [2048, 512], P('sp', 'tp'), may hold values from -0.125 to 0.125
- keys: bfloat16 [2048, 512], P('sp', 'tp'), may hold values from -0.3125 to 0.3125
- values: bfloat16 [2048, 1024], P('sp', 'tp'), may hold values from -1.5 to 1.5
- log_decay: float32 [2048, 512], P('sp', 'tp'), may hold values from -0.1 to 0, as said below
- block_states: float32 [32, 8, 64, 128], P('sp', 'tp'), may hold values from -1.75 to 1.75
Outputs:
- grad_queries: bfloat16 [2048, 512], P('sp', 'tp')
- grad_keys: bfloat16 [2048, 512], P('sp', 'tp')
- grad_values: bfloat16 [2048, 1024], P('sp', 'tp')
- grad_decay: float32 [2048, 512], P('sp', 'tp')
- grad_out_weight: float32 [1024, 2048], P('tp', 'sp')
- grad_gate_w: bfloat16 [16, 2048, 1792], P('sp', None, 'tp')
- grad_up_w: bfloat16 [16, 2048, 1792], P('sp', None, 'tp')
- grad_down_w: bfloat16 [16, 1792, 2048], P('sp', 'tp')
Inputs may be any that keep to these rules, and one draw needn't show every extreme that they name: `route_ids`: each row names two different experts. In the rows of one index of sp no expert is named more than 48 times, and in every draw some expert is named exactly 48 times by the rows of some index of sp. `log_decay`: Negative.
All inputs are finite; a program needn't handle non-finite values.
Results may differ from a plain program's by a relative error of at most 0.013.
Values may be sent and summed in bfloat16 or wider, within the bound.
A program may use at most 128 MiB of HBM per device.

v0:
```python
import functools

import jax
import jax.numpy as jnp
from jax import lax
from jax.experimental import pallas as pl
from jax.experimental.pallas import tpu as pltpu
from jax.sharding import Mesh, PartitionSpec as P

MESH = pl.DeviceIdType.MESH
SP = ("ep", "pair")

DK = 64
DV = 128
BLK = 64


PRECISE = lax.Precision.HIGHEST
ACROSS = (((1,), (1,)), ((), ()))
DOWNWARD = (((0,), (0,)), ((), ()))


def sp_size():
    return lax.axis_size("ep") * lax.axis_size("pair")


def sp_index():
    return lax.axis_index("ep") * lax.axis_size("pair") + lax.axis_index("pair")


def dispatch_kernel(
    experts, width, tok_send, grad_send, tok_out, grad_out,
    local_sem, direct_send, direct_recv, pair_send, pair_recv, core_send, core_recv,
):
    e, p, t = lax.axis_index("ep"), lax.axis_index("pair"), lax.axis_index("tp")
    barrier = pltpu.get_barrier_semaphore()
    for k in range(1, experts):
        pl.semaphore_signal(
            barrier, inc=1, device_id=(lax.rem(e + k, experts), p, t), device_id_type=MESH
        )
    pl.semaphore_signal(barrier, inc=1, device_id=(e, 1 - p, t), device_id_type=MESH)
    pl.semaphore_signal(barrier, inc=1, device_id=(e, p, 1 - t), device_id_type=MESH)
    pl.semaphore_wait(barrier, experts + 1)
    columns = pl.ds(pl.multiple_of(t * width, 128), width)
    sends, outs = (tok_send, grad_send), (tok_out, grad_out)

    def direct(a, k):
        if k == 0:
            return pltpu.make_async_copy(
                sends[a].at[e], outs[a].at[p, e, :, columns], local_sem.at[a]
            )
        dest = lax.rem(e + k, experts)
        return pltpu.make_async_remote_copy(
            src_ref=sends[a].at[dest],
            dst_ref=outs[a].at[p, e, :, columns],
            send_sem=direct_send.at[a, k],
            recv_sem=direct_recv.at[a, k],
            device_id=(dest, p, t),
            device_id_type=MESH,
        )

    def passed(a, k, which, to_pair):
        source = lax.rem(e - k + experts, experts)
        place = outs[a].at[p if which == 0 else 1 - p, source, :, columns]
        return pltpu.make_async_remote_copy(
            src_ref=place,
            dst_ref=place,
            send_sem=pair_send.at[a, k] if to_pair else core_send.at[a, which, k],
            recv_sem=pair_recv.at[a, k] if to_pair else core_recv.at[a, which, k],
            device_id=(e, 1 - p, t) if to_pair else (e, p, 1 - t),
            device_id_type=MESH,
        )

    def landed_direct(a, k):
        if k == 0:
            direct(a, 0).wait()
            return
        source = lax.rem(e - k + experts, experts)
        place = outs[a].at[p, source, :, columns]
        pltpu.make_async_remote_copy(
            src_ref=place, dst_ref=place, send_sem=direct_send.at[a, k],
            recv_sem=direct_recv.at[a, k], device_id=(source, p, t), device_id_type=MESH,
        ).wait_recv()

    def landed_passed(a, k, which, from_pair):
        source = lax.rem(e - k + experts, experts)
        own = p if which == 0 else 1 - p
        if from_pair:
            place = outs[a].at[1 - p, source, :, columns]
            sems = (pair_send.at[a, k], pair_recv.at[a, k])
        else:
            other = pl.ds(pl.multiple_of((1 - t) * width, 128), width)
            place = outs[a].at[own, source, :, other]
            sems = (core_send.at[a, which, k], core_recv.at[a, which, k])
        pltpu.make_async_remote_copy(
            src_ref=place, dst_ref=place, send_sem=sems[0], recv_sem=sems[1],
            device_id=(e, 1 - p, t), device_id_type=MESH,
        ).wait_recv()

    for a in range(2):
        for k in range(experts):
            direct(a, k).start()
    steps = [(a, k) for a in range(2) for k in range(experts)]
    lag = 2
    for i in range(len(steps) + lag):
        if i < len(steps):
            a, k = steps[i]
            landed_direct(a, k)
            passed(a, k, 0, True).start()
            passed(a, k, 0, False).start()
        if i >= lag:
            a, k = steps[i - lag]
            landed_passed(a, k, 1, True)
            passed(a, k, 1, False).start()
    for a, k in steps:
        for which in range(2):
            landed_passed(a, k, which, False)
    for a, k in steps:
        if k:
            direct(a, k).wait_send()
        passed(a, k, 0, True).wait_send()
        passed(a, k, 0, False).wait_send()
        passed(a, k, 1, False).wait_send()


def dispatch_rows(token_send, grad_send):
    experts, capacity, width = token_send.shape
    out = jax.ShapeDtypeStruct((2, experts, capacity, 2 * width), token_send.dtype)
    vmem = pl.BlockSpec(memory_space=pltpu.VMEM)
    dma = pltpu.SemaphoreType.DMA
    return pl.pallas_call(
        functools.partial(dispatch_kernel, experts, width),
        out_shape=(out, out),
        in_specs=[vmem, vmem],
        out_specs=(vmem, vmem),
        scratch_shapes=[
            dma((2,)),
            dma((2, experts)),
            dma((2, experts)),
            dma((2, experts)),
            dma((2, experts)),
            dma((2, 2, experts)),
            dma((2, 2, experts)),
        ],
        compiler_params=pltpu.CompilerParams(collective_id=0, has_side_effects=True),
        name="dispatch_rows",
    )(token_send, grad_send)


def suffix_kernel(
    count, rows, state, reach, terms, out, right, held, result, gathered,
    local_sem, go_send, go_recv, back_send, back_recv, term_send, term_recv,
):
    me = sp_index()
    t = lax.axis_index("tp")

    def place(i):
        return (lax.div(i, 2), lax.rem(i, 2), t)

    barrier = pltpu.get_barrier_semaphore()
    for k in range(1, count):
        pl.semaphore_signal(
            barrier, inc=1, device_id=place(lax.rem(me + k, count)), device_id_type=MESH
        )
    pl.semaphore_wait(barrier, count - 1)

    def go(k):
        dest = lax.rem(me + k, count)
        if k == 0:
            return pltpu.make_async_copy(state.at[me], held.at[me], local_sem.at[0])
        return pltpu.make_async_remote_copy(
            src_ref=state.at[dest], dst_ref=held.at[me], send_sem=go_send.at[k],
            recv_sem=go_recv.at[k], device_id=place(dest), device_id_type=MESH,
        )

    def back(k):
        dest = lax.rem(me + k, count)
        if k == 0:
            return pltpu.make_async_copy(result.at[me], out.at[me], local_sem.at[1])
        return pltpu.make_async_remote_copy(
            src_ref=result.at[dest], dst_ref=out.at[me], send_sem=back_send.at[k],
            recv_sem=back_recv.at[k], device_id=place(dest), device_id_type=MESH,
        )

    def landed(ref, sends, recvs, k):
        source = lax.rem(me - k + count, count)
        pltpu.make_async_remote_copy(
            src_ref=ref.at[source], dst_ref=ref.at[source], send_sem=sends.at[k],
            recv_sem=recvs.at[k], device_id=place(source), device_id_type=MESH,
        ).wait_recv()

    for k in range(count):
        go(k).start()
    go(0).wait()
    for k in range(1, count):
        landed(held, go_send, go_recv, k)
    total = jnp.zeros((rows, state.shape[-1]), jnp.float32)
    for i in range(count - 1, -1, -1):
        result[i] = total
        total = held[i, 1] * total + held[i, 0]
    for k in range(count):
        back(k).start()
    back(0).wait()
    for k in range(1, count):
        landed(out, back_send, back_recv, k)
    lanes = lax.broadcasted_iota(jnp.int32, (rows, state.shape[-1]), 1)
    places = lax.broadcasted_iota(jnp.int32, (rows, state.shape[-1]), 0)
    groups = [jnp.zeros((1, 128), jnp.float32) for _ in range(terms.shape[0])]
    for c in range(count):
        dots = jnp.sum(reach[c] * out[c], axis=1, keepdims=True)
        picked = jnp.where(lanes == places + (c * rows) % 128, dots, 0.0)
        groups[c * rows // 128] += jnp.sum(picked, axis=0, keepdims=True)
    gathered[me] = terms[...] - jnp.concatenate(groups, axis=0)

    def tell(k):
        return pltpu.make_async_remote_copy(
            src_ref=gathered.at[me], dst_ref=gathered.at[me], send_sem=term_send.at[k],
            recv_sem=term_recv.at[k], device_id=place(lax.rem(me + k, count)), device_id_type=MESH,
        )

    for k in range(1, count):
        go(k).wait_send()
        back(k).wait_send()
    for k in range(1, count):
        tell(k).start()
    for k in range(1, count):
        landed(gathered, term_send, term_recv, k)
    summed = jnp.zeros(terms.shape, jnp.float32)
    for i in range(count):
        summed += jnp.where(i > me, gathered[i], 0.0)
    right[...] = summed
    for k in range(1, count):
        tell(k).wait_send()


def suffix_states(gain, local_sum, reach_sum, terms):
    count = sp_size()
    heads, dk, dv = local_sum.shape
    rows = heads * dk // count
    packed = jnp.stack(
        [
            local_sum.reshape(count, rows, dv),
            jnp.broadcast_to(gain[:, :, None], local_sum.shape).reshape(count, rows, dv),
        ],
        axis=1,
    )
    vmem = pl.BlockSpec(memory_space=pltpu.VMEM)
    dma = pltpu.SemaphoreType.DMA
    terms = terms.reshape(heads * dk // 128, 128)
    out, right = pl.pallas_call(
        functools.partial(suffix_kernel, count, rows),
        out_shape=(
            jax.ShapeDtypeStruct((count, rows, dv), jnp.float32),
            jax.ShapeDtypeStruct(terms.shape, jnp.float32),
        ),
        in_specs=[vmem] * 3,
        out_specs=(vmem, vmem),
        scratch_shapes=[
            pltpu.VMEM((count, 2, rows, dv), jnp.float32),
            pltpu.VMEM((count, rows, dv), jnp.float32),
            pltpu.VMEM((count,) + terms.shape, jnp.float32),
            dma((2,)),
            dma((count,)),
            dma((count,)),
            dma((count,)),
            dma((count,)),
            dma((count,)),
            dma((count,)),
        ],
        compiler_params=pltpu.CompilerParams(collective_id=1, has_side_effects=True),
        name="suffix_states",
    )(packed, reach_sum.reshape(count, rows, dv), terms)
    return out.reshape(local_sum.shape), right.reshape(1, -1)


def return_kernel(
    experts, width, steps, parts, tokens, grads, hidden, d_gate, d_up,
    returned, gate_out, up_out, down_out,
    core_held, pair_stage, pair_held, send_stage, gate_stage, up_stage, down_stage,
    out_sem, local_sem, core_send, core_recv, pair_send, pair_recv, back_send, back_recv,
):
    e, p, t = lax.axis_index("ep"), lax.axis_index("pair"), lax.axis_index("tp")
    barrier = pltpu.get_barrier_semaphore()
    for k in range(1, experts):
        pl.semaphore_signal(
            barrier, inc=1, device_id=(lax.rem(e + k, experts), p, t), device_id_type=MESH
        )
    pl.semaphore_signal(barrier, inc=1, device_id=(e, 1 - p, t), device_id_type=MESH)
    pl.semaphore_signal(barrier, inc=1, device_id=(e, p, 1 - t), device_id_type=MESH)
    pl.semaphore_wait(barrier, experts + 1)
    own_columns = pl.ds(pl.multiple_of(t * width, 128), width)
    core_columns = pl.ds(pl.multiple_of((1 - t) * width, 128), width)

    def owner(k):
        return lax.rem(e + 1 + k, experts)

    def core_copy(which, k):
        side = 1 - p if which == 0 else p
        return pltpu.make_async_remote_copy(
            src_ref=parts.at[side, owner(k), :, core_columns],
            dst_ref=core_held.at[which, k],
            send_sem=core_send.at[which, k],
            recv_sem=core_recv.at[which, k],
            device_id=(e, p, 1 - t),
            device_id_type=MESH,
        )

    def pair_copy(k):
        return pltpu.make_async_remote_copy(
            src_ref=pair_stage.at[k], dst_ref=pair_held.at[k], send_sem=pair_send.at[k],
            recv_sem=pair_recv.at[k], device_id=(e, 1 - p, t), device_id_type=MESH,
        )

    def back_copy(k):
        return pltpu.make_async_remote_copy(
            src_ref=send_stage.at[k], dst_ref=returned.at[e], send_sem=back_send.at[k],
            recv_sem=back_recv.at[k], device_id=(owner(k), p, t), device_id_type=MESH,
        )

    def half_of(which, k):
        side = 1 - p if which == 0 else p
        mine = parts[side, owner(k), :, own_columns].astype(jnp.float32)
        return (mine + core_held[which, k].astype(jnp.float32)).astype(jnp.bfloat16)

    for which in range(2):
        for k in range(experts):
            core_copy(which, k).start()
    for k in range(experts):
        core_copy(0, k).wait_recv()
        pair_stage[k] = half_of(0, k)
        if k:
            pair_copy(k - 1).start()
    pair_copy(experts - 1).start()
    for k in range(experts):
        core_copy(1, k).wait_recv()

    def down_step(i, carry):
        cut = pl.ds(pl.multiple_of(i * 128, 128), 128)
        down_stage[cut, :] = lax.dot_general(
            hidden[:, cut], grads[...], DOWNWARD, preferred_element_type=jnp.float32
        ).astype(jnp.bfloat16)
        pltpu.make_async_copy(down_stage.at[cut], down_out.at[cut], out_sem.at[0]).start()
        return carry

    lax.fori_loop(0, hidden.shape[1] // 128, down_step, 0)
    span = tokens.shape[1] // steps
    each = experts // steps

    def weight_step(i, carry):
        cut = pl.ds(pl.multiple_of(i * span, span), span)
        gate_stage[cut, :] = lax.dot_general(
            tokens[:, cut], d_gate[...], DOWNWARD, preferred_element_type=jnp.float32
        ).astype(jnp.bfloat16)
        for j in range(each):
            k = i * each + j
            pair_copy(k).wait_recv()
            total = half_of(1, k).astype(jnp.float32) + pair_held[k].astype(jnp.float32)
            send_stage[k] = total.astype(jnp.bfloat16)
        up_stage[cut, :] = lax.dot_general(
            tokens[:, cut], d_up[...], DOWNWARD, preferred_element_type=jnp.float32
        ).astype(jnp.bfloat16)
        for j in range(each):
            k = i * each + j

            @pl.when(k < experts - 1)
            def _():
                back_copy(k).start()

        pltpu.make_async_copy(gate_stage.at[cut], gate_out.at[cut], out_sem.at[1]).start()
        pltpu.make_async_copy(up_stage.at[cut], up_out.at[cut], out_sem.at[2]).start()
        return carry

    lax.fori_loop(0, steps, weight_step, 0)
    own = pltpu.make_async_copy(send_stage.at[experts - 1], returned.at[e], local_sem)
    own.start()
    own.wait()
    for k in range(experts - 1):
        source = lax.rem(e - 1 - k + experts, experts)
        pltpu.make_async_remote_copy(
            src_ref=returned.at[source], dst_ref=returned.at[source], send_sem=back_send.at[k],
            recv_sem=back_recv.at[k], device_id=(source, p, t), device_id_type=MESH,
        ).wait_recv()
    for k in range(experts):
        core_copy(0, k).wait_send()
        core_copy(1, k).wait_send()
        pair_copy(k).wait_send()
        if k < experts - 1:
            back_copy(k).wait_send()
    pltpu.make_async_copy(down_stage, down_out, out_sem.at[0]).wait()
    pltpu.make_async_copy(gate_stage, gate_out, out_sem.at[1]).wait()
    pltpu.make_async_copy(up_stage, up_out, out_sem.at[2]).wait()


def return_rows(parts, tokens, grads, hidden, d_gate, d_up):
    _, experts, capacity, model_width = parts.shape
    width = model_width // 2
    units = hidden.shape[1]
    half = (experts, capacity, width)
    vmem = pl.BlockSpec(memory_space=pltpu.VMEM)
    hbm = pl.BlockSpec(memory_space=pl.ANY)
    dma = pltpu.SemaphoreType.DMA
    wide, tall = (model_width, units), (units, model_width)
    kind = jnp.bfloat16
    shape = jax.ShapeDtypeStruct
    return pl.pallas_call(
        functools.partial(return_kernel, experts, width, min(8, experts)),
        out_shape=(shape(half, kind), shape(wide, kind), shape(wide, kind), shape(tall, kind)),
        in_specs=[vmem] * 6,
        out_specs=(vmem, hbm, hbm, hbm),
        scratch_shapes=[
            pltpu.VMEM((2,) + half, kind),
            pltpu.VMEM(half, kind),
            pltpu.VMEM(half, kind),
            pltpu.VMEM(half, kind),
            pltpu.VMEM(wide, kind),
            pltpu.VMEM(wide, kind),
            pltpu.VMEM(tall, kind),
            dma((3,)),
            dma,
            dma((2, experts)),
            dma((2, experts)),
            dma((experts,)),
            dma((experts,)),
            dma((experts,)),
            dma((experts,)),
        ],
        compiler_params=pltpu.CompilerParams(
            collective_id=2, has_side_effects=True, vmem_limit_bytes=60 * 1024 * 1024
        ),
        name="return_rows",
    )(parts, tokens, grads, hidden, d_gate, d_up)


def block_back(carried, inputs):
    q_block, k_block, v_block, o_block, decay_block, state_in = inputs
    cumul = jnp.cumsum(decay_block, axis=0)
    block_total = cumul[-1]
    growth = jnp.exp(cumul)
    shrink = jnp.exp(-cumul)
    to_end = jnp.exp(block_total[None] - cumul)
    span_len = q_block.shape[0]
    causal = (jnp.arange(span_len)[:, None] >= jnp.arange(span_len)[None, :]).astype(jnp.float32)
    q_grow = q_block * growth
    k_shrink = k_block * shrink
    scores = jnp.einsum("thv,shv->hts", o_block, v_block, precision=PRECISE) * causal
    mutual = jnp.einsum("thd,shd->hts", q_grow, k_shrink, precision=PRECISE) * causal
    grad_q = growth * (
        jnp.einsum("thv,hdv->thd", o_block, state_in, precision=PRECISE)
        + jnp.einsum("hts,shd->thd", scores, k_shrink, precision=PRECISE)
    )
    grad_k = to_end * jnp.einsum(
        "hdv,shv->shd", carried, v_block, precision=PRECISE
    ) + shrink * jnp.einsum("hts,thd->shd", scores, q_grow, precision=PRECISE)
    grad_v = jnp.einsum("shd,hdv->shv", k_block * to_end, carried, precision=PRECISE) + jnp.einsum(
        "hts,thv->shv", mutual, o_block, precision=PRECISE
    )
    contrib = q_block * grad_q - k_block * grad_k
    carried = jnp.exp(block_total)[:, :, None] * carried + jnp.einsum(
        "thd,thv->hdv", q_grow, o_block, precision=PRECISE
    )
    return (carried, (grad_q, grad_k, grad_v, contrib))


def body(
    moe_input,
    out_grad,
    route_ids,
    route_weights,
    gate_w,
    up_w,
    down_w,
    mixer_out,
    out_weight,
    queries,
    keys,
    values,
    log_decay,
    block_states,
):
    sp_count = sp_size()
    experts = lax.axis_size("ep")
    tok_rows = moe_input.shape[0]
    model_width = moe_input.shape[1]
    capacity = 3 * tok_rows // experts
    flat_ids = route_ids.reshape(-1)
    one_hot = (flat_ids[:, None] == jnp.arange(experts, dtype=jnp.int32)[None, :]).astype(jnp.int32)
    earlier_count = jnp.sum(jnp.cumsum(one_hot, axis=0) * one_hot, axis=1) - 1
    slot_index = flat_ids * capacity + earlier_count
    dispatch = (
        jnp.arange(experts * capacity, dtype=jnp.int32)[:, None] == slot_index[None, :]
    ).astype(jnp.bfloat16)
    token_pick = jnp.sum(dispatch.reshape(experts * capacity, tok_rows, 2), axis=2)
    col_count = model_width // lax.axis_size("tp")
    col_start = lax.axis_index("tp") * col_count
    source_tokens = lax.dynamic_slice_in_dim(moe_input, col_start, col_count, 1)
    source_grads = lax.dynamic_slice_in_dim(out_grad, col_start, col_count, 1)
    send_width = source_tokens.shape[1]
    scaled = (route_weights[:, :, None] * source_grads[:, None, :].astype(jnp.float32)).astype(
        jnp.bfloat16
    )
    scaled = scaled.reshape(2 * tok_rows, send_width)
    token_send = jnp.dot(token_pick, source_tokens, preferred_element_type=jnp.float32).astype(
        jnp.bfloat16
    )
    grad_send = jnp.dot(dispatch, scaled, preferred_element_type=jnp.float32).astype(jnp.bfloat16)

    arrived_tokens, arrived_grads = dispatch_rows(
        token_send.reshape(experts, capacity, send_width),
        grad_send.reshape(experts, capacity, send_width),
    )
    arrived_tokens = arrived_tokens.reshape(sp_count * capacity, model_width)
    arrived_grads = arrived_grads.reshape(sp_count * capacity, model_width)
    gate_mat = gate_w[0]
    up_mat = up_w[0]
    down_mat = down_w[0]
    gate_pre = jnp.dot(arrived_tokens, gate_mat, preferred_element_type=jnp.float32)
    up_pre = jnp.dot(arrived_tokens, up_mat, preferred_element_type=jnp.float32)
    sigmoid_gate = jax.nn.sigmoid(gate_pre)
    hidden = (gate_pre * sigmoid_gate * up_pre).astype(jnp.bfloat16)
    d_hidden = lax.dot_general(arrived_grads, down_mat, ACROSS, preferred_element_type=jnp.float32)
    d_up = (d_hidden * gate_pre * sigmoid_gate).astype(jnp.bfloat16)
    d_gate = (d_hidden * up_pre * sigmoid_gate * (1.0 + gate_pre * (1.0 - sigmoid_gate))).astype(
        jnp.bfloat16
    )
    partial_value = lax.dot_general(
        d_gate, gate_mat, ACROSS, preferred_element_type=jnp.float32
    ) + lax.dot_general(d_up, up_mat, ACROSS, preferred_element_type=jnp.float32)
    parts = partial_value.astype(jnp.bfloat16)
    returned, grad_gate, grad_up, grad_down = return_rows(
        parts.reshape(2, experts, capacity, model_width),
        arrived_tokens,
        arrived_grads,
        hidden,
        d_gate,
        d_up,
    )
    returned = returned.reshape(experts * capacity, col_count)
    moe_grad = lax.dot_general(token_pick, returned, DOWNWARD, preferred_element_type=jnp.float32)
    grad_mid = (source_grads.astype(jnp.float32) + moe_grad).astype(jnp.bfloat16)
    grad_mid = lax.all_gather(grad_mid, "tp", axis=1, tiled=True)
    mixer_all = lax.all_gather(mixer_out, SP, axis=0, tiled=True)
    mid_columns = lax.all_to_all(grad_mid, SP, split_axis=1, concat_axis=0, tiled=True)
    grad_out_weight = lax.dot_general(
        mixer_all, mid_columns, DOWNWARD, preferred_element_type=jnp.float32
    )
    grad_mixed = lax.dot_general(
        grad_mid, out_weight, ACROSS, preferred_element_type=jnp.float32
    ).astype(jnp.bfloat16)
    heads_local = queries.shape[1] // DK
    blocks = tok_rows // BLK

    def shaped(array, depth):
        return array.astype(jnp.float32).reshape(blocks, BLK, heads_local, depth)

    q_blocks = shaped(queries, DK)
    k_blocks = shaped(keys, DK)
    v_blocks = shaped(values, DV)
    decay_blocks = shaped(log_decay, DK)
    inputs = (q_blocks, k_blocks, v_blocks, shaped(grad_mixed, DV), decay_blocks, block_states)
    zero_state = jnp.zeros((heads_local, DK, DV), jnp.float32)
    local_sum, (grad_q, grad_k, grad_v, contrib) = lax.scan(
        block_back, zero_state, inputs, reverse=True
    )
    cumul = jnp.cumsum(decay_blocks, axis=1)
    totals = cumul[:, -1]
    offsets = jnp.cumsum(totals, axis=0) - totals
    position = cumul + offsets[:, None]
    device_total = jnp.sum(totals, axis=0)
    fade_out = jnp.exp(device_total[None, None] - position)
    k_fade = k_blocks * fade_out
    reach_sum = jnp.einsum("nshd,nshv->hdv", k_fade, v_blocks, precision=PRECISE)
    from_right, right_terms = suffix_states(
        jnp.exp(device_total), local_sum, reach_sum, jnp.sum(contrib, axis=(0, 1))
    )
    key_part = jnp.einsum("nshv,hdv->nshd", v_blocks, from_right, precision=PRECISE)
    grad_k = grad_k + fade_out * key_part
    grad_v = grad_v + jnp.einsum("nshd,hdv->nshv", k_fade, from_right, precision=PRECISE)
    contrib = (contrib - k_fade * key_part).reshape(tok_rows, heads_local * DK)
    grad_decay = jnp.flip(jnp.cumsum(jnp.flip(contrib, 0), axis=0), 0) + right_terms
    return (
        grad_q.reshape(tok_rows, heads_local * DK).astype(jnp.bfloat16),
        grad_k.reshape(tok_rows, heads_local * DK).astype(jnp.bfloat16),
        grad_v.reshape(tok_rows, heads_local * DV).astype(jnp.bfloat16),
        grad_decay,
        grad_out_weight,
        grad_gate[None],
        grad_up[None],
        grad_down[None],
    )


def solution(mesh):
    sp_count, tp_count = mesh.devices.shape
    mesh = Mesh(mesh.devices.reshape(sp_count // 2, 2, tp_count), ("ep", "pair", "tp"))
    placed = (
        P(SP, None),
        P(SP, None),
        P(SP, None),
        P(SP, None),
        P(SP, None, "tp"),
        P(SP, None, "tp"),
        P(SP, "tp", None),
        P(SP, "tp"),
        P("tp", None),
        P(SP, "tp"),
        P(SP, "tp"),
        P(SP, "tp"),
        P(SP, "tp"),
        P(SP, "tp", None, None),
    )
    return jax.shard_map(
        body,
        mesh=mesh,
        in_specs=placed,
        out_specs=(
            P(SP, "tp"),
            P(SP, "tp"),
            P(SP, "tp"),
            P(SP, "tp"),
            P("tp", SP),
            P(SP, None, "tp"),
            P(SP, None, "tp"),
            P(SP, "tp", None),
        ),
        check_vma=False,
    )
```

profile of v0, /device:TPU:0, one launch (start us, length us, event | category | flops | bytes accessed | tf_op | source)
XLA Modules:
  0.0 242.2 jit_solution(13476946105849944110)
XLA Ops:
  11.3 1.3 mul.208
  12.7 1.9 mul.209
  14.9 2.2 convolution_convert_fusion.1
  17.1 1.3 convolution_convert_fusion
  18.4 53.1 %dispatch_rows.1 = (bf16[2,8,48,2048]{3,2,1,0:T(8,128)(2,1)}, bf16[2,8,48,2048]{3,2,1,0:T(8,128)(2,1)}) custom-call(bf16[8,48,1024]{2,1,0:T(8,128)(2,1)} %bitcast.227, bf16[8,48,1024]{2,1,0:T(8,128)(2,1)} %bitcast.228), custom_call_target="tpu_custom_call" | custom-call | tf_op jit(solution)/shard_map/dispatch_rows/pallas_call | solution.py:131
  71.6 6.5 %fusion.30 = f32[768,896]{1,0:T(8,128)S(1)} fusion(bf16[768,2048]{1,0:T(8,128)(2,1)} %bitcast.229, bf16[1,2048,896]{2,1,0:T(8,128)(2,1)} %param.20), kind=kOutput, calls=%fused_computation.57 | convolution fusion | flops 2818572288 | bytes 9568256 | tf_op jit(solution)/shard_map/dot_general | solution.py:516
  78.2 3.5 %fusion.36 = f32[768,896]{1,0:T(8,128)S(1)} fusion(bf16[768,2048]{1,0:T(8,128)(2,1)S(1)} %bitcast.233, bf16[1,896,2048]{2,1,0:T(8,128)(2,1)S(1)} %copy-done.19), kind=kOutput, calls=%fused_computation.63 | convolution fusion | flops 2818572288 | bytes 9568256 | tf_op jit(solution)/shard_map/dot_general | solution.py:520
  81.8 5.3 %multiply_convert_fusion = (bf16[768,896]{1,0:T(8,128)(2,1)}, bf16[768,896]{1,0:T(8,128)(2,1)S(1)}, bf16[768,896]{1,0:T(8,128)(2,1)S(1)}) fusion(f32[768,896]{1,0:T(8,128)S(1)} %fusion.30, f32[768,896]{1,0:T(8,128)S(1)} %fusion.36, bf16[768,2048]{1,0:T(8,128)(2,1)S(1)} %bitcast.231, bf16[1,2048,896]{2,1,0:T(8,128)(2,1)S(1)} %copy-done.21), kind=kOutput, calls=%fused_computation.65 | convolution fusion | flops 2829582336 | bytes 16449536 | tf_op jit(solution)/shard_map/dot_general | solution.py:517
  87.1 3.4 %fusion.28 = f32[768,2048]{1,0:T(8,128)S(1)} fusion(bf16[768,896]{1,0:T(8,128)(2,1)S(1)} %get-tuple-element.420.d_gate, bf16[1,2048,896]{2,1,0:T(8,128)(2,1)S(1)} %copy-done.20), kind=kOutput, calls=%fused_computation.55 | convolution fusion | flops 2818572288 | bytes 11337728 | tf_op jit(solution)/shard_map/dot_general | solution.py:525
  90.5 5.0 %add_convert_fusion = bf16[768,2048]{1,0:T(8,128)(2,1)} fusion(f32[768,2048]{1,0:T(8,128)S(1)} %fusion.28, bf16[768,896]{1,0:T(8,128)(2,1)S(1)} %get-tuple-element.421.d_up, bf16[1,2048,896]{2,1,0:T(8,128)(2,1)S(1)} %copy-done.21), kind=kOutput, calls=%fused_computation.54 | convolution fusion | flops 2821718016 | bytes 14483456 | tf_op jit(solution)/shard_map/dot_general | solution.py:527
  95.6 39.8 %return_rows.1 = (bf16[8,48,1024]{2,1,0:T(8,128)(2,1)}, bf16[2048,896]{1,0:T(8,128)(2,1)}, bf16[2048,896]{1,0:T(8,128)(2,1)}, bf16[896,2048]{1,0:T(8,128)(2,1)}) custom-call(bf16[2,8,48,2048]{3,2,1,0:T(8,128)(2,1)} %bitcast.234, bf16[768,2048]{1,0:T(8,128)(2,1)} %bitcast.230, bf16[768,2048]{1,0:T(8,128)(2,1)} %bitcast.232, ...), custom_call_target="tpu_custom_call" | custom-call | tf_op jit(solution)/shard_map/return_rows/pallas_call | solution.py:405
  135.4 1.5 fusion.40
  136.9 2.2 all_gather.6
  140.0 10.0 %all-to-all-start = ((bf16[128,16,128]{2,0,1:T(8,128)(2,1)}), bf16[128,16,128]{2,0,1:T(8,128)(2,1)}, u32[]{:S(2)}, u32[]{:S(2)}) async-start(bf16[128,16,128]{2,0,1:T(8,128)(2,1)} %copy_bitcast_fusion.8), calls=%async_computation | async-start | bytes 1048576 | tf_op jit(solution)/shard_map/all_to_all | solution.py:542
  158.6 18.9 %while.23 = (s32[]{:T(128)}, f32[4,64,128]{2,1,0:T(8,128)S(1)}, bf16[2,64,4,64]{1,3,2,0:T(8,128)(2,1)}, f32[2,64,4,64]{1,3,0,2:T(8,128)}, f32[2,64,4,128]{3,1,0,...) while((s32[]{:T(128)}, f32[4,64,128]{2,1,0:T(8,128)S(1)}, ...), condition=%wide.region_6.7_spmd.clone, body=%wide.region_4.6_spmd.clone.sunk | while | flops 190324736 | bytes 5430457 | solution.py:561
  180.2 1.8 fusion.50
  183.8 29.4 %suffix_states.1 = (f32[16,16,128]{2,1,0:T(8,128)}, f32[2,128]{1,0:T(2,128)}) custom-call(f32[16,2,16,128]{3,2,1,0:T(8,128)} %pad_maximum_fusion.state, f32[16,16,128]{2,1,0:T(8,128)} %bitcast.238, f32[2,128]{1,0:T(2,128)} %reshape.184.terms), custom_call_target="tpu_custom_call" | custom-call | tf_op jit(solution)/shard_map/suffix_states/pallas_call | solution.py:250
  213.2 2.3 copy_subtract_fusion
  217.2 1.3 fusion.57
  222.8 2.2 convolution_bitcast_fusion.4
  225.9 4.3 %copy.220 = bf16[1,2048,896]{2,1,0:T(8,128)(2,1)} copy(bf16[1,2048,896]{2,1,0:T(8,128)(2,1)} %bitcast.226) | data formatting | bytes 7340032
  230.2 1.9 copy.221
  232.0 1.5 copy-done.1
  233.5 1.8 copy.222
  (143 shorter events, 43.7 us)
Async XLA Ops:
  7.2 144.2 %copy-start = (bf16[512,2048]{1,0:T(8,128)(2,1)S(1)}, bf16[512,2048]{1,0:T(8,128)(2,1)}, u32[]{:S(2)}) copy-start(bf16[512,2048]{1,0:T(8,128)(2,1)} %param.24) | copy-start | bytes 6291460
  7.2 7.4 %copy-start.17 = (f32[128,2]{0,1:T(2,128)S(1)}, f32[128,2]{0,1:T(2,128)}, u32[]{:S(2)}) copy-start(f32[128,2]{0,1:T(2,128)} %param.19) | copy-start | bytes 3076
  71.6 6.6 %copy-start.4 = (bf16[2,8,48,2048]{3,2,1,0:T(8,128)(2,1)S(1)}, bf16[2,8,48,2048]{3,2,1,0:T(8,128)(2,1)}, u32[]{:S(2)}) copy-start(bf16[2,8,48,2048]{3,2,1,0:T(8,128)(2,1)} %get-tuple-element.256) | copy-start | bytes 9437188
  71.6 6.6 %copy-start.19 = (bf16[1,896,2048]{2,1,0:T(8,128)(2,1)S(1)}, bf16[1,896,2048]{2,1,0:T(8,128)(2,1)}, u32[]{:S(2)}) copy-start(bf16[1,896,2048]{2,1,0:T(8,128)(2,1)} %param.22) | copy-start | bytes 11010052
  78.1 3.6 %copy-start.3 = (bf16[2,8,48,2048]{3,2,1,0:T(8,128)(2,1)S(1)}, bf16[2,8,48,2048]{3,2,1,0:T(8,128)(2,1)}, u32[]{:S(2)}) copy-start(bf16[2,8,48,2048]{3,2,1,0:T(8,128)(2,1)} %get-tuple-element.257) | copy-start | bytes 9437188
  78.2 3.6 %copy-start.21 = (bf16[1,2048,896]{2,1,0:T(8,128)(2,1)S(1)}, bf16[1,2048,896]{2,1,0:T(8,128)(2,1)}, u32[]{:S(2)}) copy-start(bf16[1,2048,896]{2,1,0:T(8,128)(2,1)} %param.21) | copy-start | bytes 11010052
  81.7 5.3 %copy-start.20 = (bf16[1,2048,896]{2,1,0:T(8,128)(2,1)S(1)}, bf16[1,2048,896]{2,1,0:T(8,128)(2,1)}, u32[]{:S(2)}) copy-start(bf16[1,2048,896]{2,1,0:T(8,128)(2,1)} %param.20) | copy-start | bytes 11010052
  87.1 3.5 %copy-start.8 = (bf16[768,896]{1,0:T(8,128)(2,1)}, bf16[768,896]{1,0:T(8,128)(2,1)S(1)}, u32[]{:S(2)}) copy-start(bf16[768,896]{1,0:T(8,128)(2,1)S(1)} %get-tuple-element.420.d_gate) | copy-start | bytes 4128772
  87.1 3.5 %copy-start.9 = (bf16[768,896]{1,0:T(8,128)(2,1)}, bf16[768,896]{1,0:T(8,128)(2,1)S(1)}, u32[]{:S(2)}) copy-start(bf16[768,896]{1,0:T(8,128)(2,1)S(1)} %get-tuple-element.421.d_up) | copy-start | bytes 4128772
  95.5 39.8 %copy-start.10 = (bf16[128,2048]{1,0:T(8,128)(2,1)S(1)}, bf16[128,2048]{1,0:T(8,128)(2,1)}, u32[]{:S(2)}) copy-start(bf16[128,2048]{1,0:T(8,128)(2,1)} %param.17) | copy-start | bytes 1572868
  139.0 14.0 %copy-start.14 = (bf16[128,512]{1,0:T(8,128)(2,1)S(1)}, bf16[128,512]{1,0:T(8,128)(2,1)}, u32[]{:S(2)}) copy-start(bf16[128,512]{1,0:T(8,128)(2,1)} %param.27) | copy-start | bytes 393220
  140.0 13.8 %copy-start.13 = (f32[128,256]{1,0:T(8,128)S(1)}, f32[128,256]{1,0:T(8,128)}, u32[]{:S(2)}) copy-start(f32[128,256]{1,0:T(8,128)} %param.28) | copy-start | bytes 393220
  140.0 14.7 %copy-start.15 = (bf16[128,256]{1,0:T(8,128)(2,1)S(1)}, bf16[128,256]{1,0:T(8,128)(2,1)}, u32[]{:S(2)}) copy-start(bf16[128,256]{1,0:T(8,128)(2,1)} %param.26) | copy-start | bytes 196612
  140.0 82.8 %all-to-all-start = ((bf16[128,16,128]{2,0,1:T(8,128)(2,1)}), bf16[128,16,128]{2,0,1:T(8,128)(2,1)}, u32[]{:S(2)}, u32[]{:S(2)}) async-start(bf16[128,16,128]{2,0,1:T(8,128)(2,1)} %copy_bitcast_fusion.8), calls=%async_computation | async-start | bytes 1048576 | tf_op jit(solution)/shard_map/all_to_all | solution.py:542
  149.9 5.6 %copy-start.16 = (bf16[128,256]{1,0:T(8,128)(2,1)S(1)}, bf16[128,256]{1,0:T(8,128)(2,1)}, u32[]{:S(2)}) copy-start(bf16[128,256]{1,0:T(8,128)(2,1)} %param.25) | copy-start | bytes 196612
  150.0 72.8 %all-gather.2.cloned.1.call-start = ((), (), s32[]{:S(2)}) async-start(), calls=%async_computation.1 | async-start | bytes 2228224 | tf_op jit(solution)/shard_map/all_gather | solution.py:541
  153.0 5.6 %copy-start.6 = (bf16[2,64,4,128]{3,2,1,0:T(4,128)(2,1)}, bf16[2,64,4,128]{3,2,1,0:T(4,128)(2,1)S(1)}, u32[]{:S(2)}) copy-start(bf16[2,64,4,128]{3,2,1,0:T(4,128)(2,1)S(1)} %reshape.181) | copy-start | bytes 393220
  177.5 5.4 %copy-start.5 = (f32[2,64,4,64]{1,3,2,0:T(8,128)S(1)}, f32[2,64,4,64]{1,3,2,0:T(8,128)}, u32[]{:S(2)}) copy-start(f32[2,64,4,64]{1,3,2,0:T(8,128)} %get-tuple-element.262) | copy-start | bytes 393220
  177.6 35.6 %copy-start.7 = (bf16[2,64,4,128]{3,2,1,0:T(4,128)(2,1)S(1)}, bf16[2,64,4,128]{3,2,1,0:T(4,128)(2,1)}, u32[]{:S(2)}) copy-start(bf16[2,64,4,128]{3,2,1,0:T(4,128)(2,1)} %copy-done.6) | copy-start | bytes 393220
  213.2 8.0 %copy-start.11 = (bf16[2,64,4,64]{1,3,2,0:T(8,128)(2,1)S(1)}, bf16[2,64,4,64]{1,3,2,0:T(8,128)(2,1)}, u32[]{:S(2)}) copy-start(bf16[2,64,4,64]{1,3,2,0:T(8,128)(2,1)} %get-tuple-element.259) | copy-start | bytes 196612
  213.2 8.9 %copy-start.18 = (f32[2,128]{1,0:T(2,128)S(1)}, f32[2,128]{1,0:T(2,128)}, u32[]{:S(2)}) copy-start(f32[2,128]{1,0:T(2,128)} %get-tuple-element.265) | copy-start | bytes 3076
  215.5 4.7 %copy-start.12 = (bf16[2,64,4,64]{1,3,0,2:T(8,128)(2,1)S(1)}, bf16[2,64,4,64]{1,3,0,2:T(8,128)(2,1)}, u32[]{:S(2)}) copy-start(bf16[2,64,4,64]{1,3,0,2:T(8,128)(2,1)} %get-tuple-element.423) | copy-start | bytes 196612
  225.9 4.3 %copy-start.2 = (bf16[2048,896]{1,0:T(8,128)(2,1)S(1)}, bf16[2048,896]{1,0:T(8,128)(2,1)}, u32[]{:S(2)}) copy-start(bf16[2048,896]{1,0:T(8,128)(2,1)} %get-tuple-element.267) | copy-start | bytes 11010052
  230.2 3.4 %copy-start.1 = (bf16[896,2048]{1,0:T(8,128)(2,1)S(1)}, bf16[896,2048]{1,0:T(8,128)(2,1)}, u32[]{:S(2)}) copy-start(bf16[896,2048]{1,0:T(8,128)(2,1)} %get-tuple-element.268) | copy-start | bytes 11010052
Sparse Core Ops, SparseCore 0:
  153.5 62.7 all-gather.1
where the time goes:
time: 243 us; the launch traced here: 242 us
  Pallas kernels  122 us (50%)
  matrix products  48.2 us (20%)
  local copies, waits for them, and re-layouts  34.4 us (14%)
  between operations  14.5 us (6%)
  starting transfers between devices  10 us (4%)
  other arithmetic  9.75 us (4%)
    pallas_call x1, Pallas kernels, dispatch_rows(): pl.pallas_call(functools.partial(dispatch_kernel, experts, width), out_sh...  53.1 us
    pallas_call x1, Pallas kernels, return_rows(): pl.pallas_call(functools.partial(return_kernel, experts, width, min(8, ex...  39.8 us
    pallas_call x1, Pallas kernels, suffix_states(): pl.pallas_call(functools.partial(suffix_kernel, count, rows), out_shape=(...  29.4 us
    unnamed x51, local copies, waits for them, and re-layouts  12.2 us
    all_to_all x1, starting transfers between devices, body(): lax.all_to_all(grad_mid, SP, split_axis=1, concat_axis=0, tiled=True)  9.96 us
    dot_general x1, matrix products, body(): jnp.dot(arrived_tokens, gate_mat, preferred_element_type=jnp.float32)  6.53 us
    dot_general x1, matrix products, body(): up_pre = jnp.dot(arrived_tokens, up_mat, preferred_element_type=jnp.float32)  5.31 us
    dot_general x1, matrix products, body(): lax.dot_general(d_up, up_mat, ACROSS, preferred_element_type=jnp.float32)  5.01 us
  transfers between devices with their start and end apart: 2, of which 0 were waited for; matrix products, arithmetic and copies ran while one was open for 17% of the time, Pallas kernels for 12%

commit v1 on v0

v1 whole, which is shorter than its diff:
```python
import functools

import jax
import jax.numpy as jnp
from jax import lax
from jax.experimental import pallas as pl
from jax.experimental.pallas import tpu as pltpu
from jax.sharding import Mesh, PartitionSpec as P

MESH = pl.DeviceIdType.MESH
SP = ("ep", "pair")

DK = 64
DV = 128
BLK = 64
PER_GROUP = 2


PRECISE = lax.Precision.HIGHEST
ACROSS = (((1,), (1,)), ((), ()))
DOWNWARD = (((0,), (0,)), ((), ()))
PLAIN = (((1,), (0,)), ((), ()))


def sp_size():
    return lax.axis_size("ep") * lax.axis_size("pair")


def sp_index():
    return lax.axis_index("ep") * lax.axis_size("pair") + lax.axis_index("pair")


def experts_kernel(
    experts, cap, ids, route_weights, moe_input, out_grad, gate_w, up_w, down_w,
    returned, gate_out, up_out, down_out,
    toks, grads, hidden, d_both, gate_up, down, silu_part, slope_part, parts, rank, tok_send,
    grad_send, core_held, pair_stage, pair_held, send_stage, gate_stage, up_stage, down_stage,
    weight_sem, out_sem, direct_send, direct_recv, pass_send, pass_recv, mate_send, mate_recv,
    core_send, core_recv, pair_send, pair_recv, back_send, back_recv,
):
    e, p, t = lax.axis_index("ep"), lax.axis_index("pair"), lax.axis_index("tp")
    f32, bf16 = jnp.float32, jnp.bfloat16
    tokens, model_width = moe_input.shape
    width = model_width // 2
    units = hidden.shape[1]
    group_rows = PER_GROUP * 2 * cap
    groups = experts // PER_GROUP
    pair_id, mate_id = (e, 1 - p, t), (e, p, 1 - t)
    barrier = pltpu.get_barrier_semaphore()
    for k in range(1, experts):
        pl.semaphore_signal(
            barrier, inc=1, device_id=(lax.rem(e + k, experts), p, t), device_id_type=MESH
        )
    pl.semaphore_signal(barrier, inc=1, device_id=pair_id, device_id_type=MESH)
    pl.semaphore_signal(barrier, inc=1, device_id=mate_id, device_id_type=MESH)
    loads = (
        pltpu.make_async_copy(gate_w, gate_up.at[:, pl.ds(0, units)], weight_sem.at[0]),
        pltpu.make_async_copy(up_w, gate_up.at[:, pl.ds(units, units)], weight_sem.at[1]),
        pltpu.make_async_copy(down_w, down, weight_sem.at[2]),
    )
    for load in loads:
        load.start()
    own_columns = pl.ds(pl.multiple_of(t * width, 128), width)
    core_columns = pl.ds(pl.multiple_of((1 - t) * width, 128), width)
    arrived = (toks, grads)
    sends = (tok_send, grad_send)

    def block(k, side):
        return pl.ds(pl.multiple_of((k * 2 + side) * cap, cap), cap)

    def remote(src, dst, send, recv, device):
        return pltpu.make_async_remote_copy(
            src_ref=src, dst_ref=dst, send_sem=send, recv_sem=recv, device_id=device,
            device_id_type=MESH,
        )

    def direct(a, k):
        return remote(
            sends[a].at[k], arrived[a].at[block(k, p), own_columns], direct_send.at[a, k],
            direct_recv.at[a, k], (lax.rem(e + k, experts), p, t),
        )

    def to_pair(a, k, side):
        place = arrived[a].at[block(k, side), own_columns]
        return remote(place, place, pass_send.at[a, k], pass_recv.at[a, k], pair_id)

    def to_mate(a, k, side, which, columns):
        place = arrived[a].at[block(k, side), columns]
        return remote(place, place, mate_send.at[a, which, k], mate_recv.at[a, which, k], mate_id)

    first_id, second_id = ids[0:1], ids[1:2]
    first_w, second_w = route_weights[0:1], route_weights[1:2]
    expert_row = lax.broadcasted_iota(jnp.int32, (experts, tokens), 0)
    member = (expert_row == first_id) | (expert_row == second_id)
    row = lax.broadcasted_iota(jnp.int32, (tokens, tokens), 0)
    col = lax.broadcasted_iota(jnp.int32, (tokens, tokens), 1)
    before = (row < col).astype(bf16)
    count = lax.dot_general(
        member.astype(f32).astype(bf16), before, PLAIN, preferred_element_type=f32
    )
    rank[...] = jnp.where(member, count.astype(jnp.int32), -1)
    spot = lax.broadcasted_iota(jnp.int32, (cap, tokens), 0)

    def rows_for(dest):
        pick = spot == rank[pl.ds(dest, 1)]
        weight = jnp.where(first_id == dest, first_w, second_w)
        scale = jnp.sum(jnp.where(pick, weight, 0.0), axis=1, keepdims=True)
        chosen = pick.astype(f32).astype(bf16)
        tok = lax.dot_general(chosen, moe_input[:, own_columns], PLAIN, preferred_element_type=f32)
        grad = lax.dot_general(chosen, out_grad[:, own_columns], PLAIN, preferred_element_type=f32)
        return tok.astype(bf16), (scale * grad).astype(bf16)

    own_tok, own_grad = rows_for(e)
    toks[block(0, p), own_columns] = own_tok
    grads[block(0, p), own_columns] = own_grad
    pl.semaphore_wait(barrier, experts + 1)
    for a in range(2):
        to_pair(a, 0, p).start()
        to_mate(a, 0, p, 0, own_columns).start()

    def send_step(k, carry):
        tok, grad = rows_for(lax.rem(e + k, experts))
        tok_send[k] = tok
        grad_send[k] = grad
        direct(0, k).start()
        direct(1, k).start()
        return carry

    lax.fori_loop(1, experts, send_step, 0)
    for load in loads:
        load.wait()

    def from_direct(a, k):
        @pl.when(k > 0)
        def _():
            direct(a, k).wait_recv()
            to_pair(a, k, p).start()
            to_mate(a, k, p, 0, own_columns).start()

    def from_pair(a, k):
        to_pair(a, k, 1 - p).wait_recv()
        to_mate(a, k, 1 - p, 1, own_columns).start()

    def from_mate(a, k):
        to_mate(a, k, p, 0, core_columns).wait_recv()
        to_mate(a, k, 1 - p, 1, core_columns).wait_recv()

    def core_copy(which, k):
        side = 1 - p if which == 0 else p
        return remote(
            parts.at[block(k, side), core_columns], core_held.at[which, k],
            core_send.at[which, k], core_recv.at[which, k], mate_id,
        )

    def pair_copy(k):
        return remote(
            pair_stage.at[k], pair_held.at[k], pair_send.at[k], pair_recv.at[k], pair_id
        )

    def back_copy(k):
        owner = lax.rem(e - k + experts, experts)
        return remote(
            send_stage.at[k], returned.at[e], back_send.at[k], back_recv.at[k], (owner, p, t)
        )

    def half_of(which, k):
        side = 1 - p if which == 0 else p
        mine = parts[block(k, side), own_columns].astype(f32)
        return (mine + core_held[which, k].astype(f32)).astype(bf16)

    def members(g):
        return [g * PER_GROUP + j for j in range(PER_GROUP)]

    def half_step(g):
        for k in members(g):
            core_copy(0, k).wait_recv()
            pair_stage[k] = half_of(0, k)
            pair_copy(k).start()

    def total_step(g):
        for k in members(g):
            core_copy(1, k).wait_recv()
            pair_copy(k).wait_recv()
            total = half_of(1, k).astype(f32) + pair_held[k].astype(f32)
            send_stage[k] = total.astype(bf16)

            @pl.when(k > 0)
            def _():
                back_copy(k).start()

    def group_step(g, carry):
        now, last = members(g), members(g - 1)
        rows = pl.ds(pl.multiple_of((g - 1) * group_rows, group_rows), group_rows)
        here, behind = g < groups, g > 0

        @pl.when(here)
        def _():
            for k in now:
                from_direct(0, k)

        @pl.when(behind)
        def _():
            for k in last:
                from_mate(0, k)
            gate_pre = lax.dot_general(
                toks[rows], gate_up[:, :units], PLAIN, preferred_element_type=f32
            )
            gate = jax.nn.sigmoid(gate_pre)
            silu_part[...] = gate_pre * gate
            slope_part[...] = gate * (1.0 + gate_pre * (1.0 - gate))

        @pl.when(here)
        def _():
            for k in now:
                from_direct(1, k)
                from_pair(0, k)

        @pl.when(behind)
        def _():
            up_pre = lax.dot_general(
                toks[rows], gate_up[:, units:], PLAIN, preferred_element_type=f32
            )
            hidden[rows] = (silu_part[...] * up_pre).astype(bf16)
            slope_part[...] = slope_part[...] * up_pre
            for k in last:
                from_mate(1, k)

        @pl.when(here)
        def _():
            for k in now:
                from_pair(1, k)

        @pl.when(behind)
        def _():
            d_hidden = lax.dot_general(grads[rows], down[...], ACROSS, preferred_element_type=f32)
            d_both[rows, :units] = (d_hidden * slope_part[...]).astype(bf16)
            d_both[rows, units:] = (d_hidden * silu_part[...]).astype(bf16)
            parts[rows, core_columns] = lax.dot_general(
                d_both[rows], gate_up[core_columns], ACROSS, preferred_element_type=f32
            ).astype(bf16)
            for k in last:
                core_copy(0, k).start()
                core_copy(1, k).start()

        @pl.when(g > 1)
        def _():
            total_step(g - 2)

        @pl.when(behind)
        def _():
            parts[rows, own_columns] = lax.dot_general(
                d_both[rows], gate_up[own_columns], ACROSS, preferred_element_type=f32
            ).astype(bf16)
            half_step(g - 1)

        return carry

    lax.fori_loop(0, groups + 1, group_step, 0)

    def down_step(i, carry):
        cut = pl.ds(pl.multiple_of(i * 128, 128), 128)
        down_stage[cut, :] = lax.dot_general(
            hidden[:, cut], grads[...], DOWNWARD, preferred_element_type=f32
        ).astype(bf16)
        pltpu.make_async_copy(down_stage.at[cut], down_out.at[cut], out_sem.at[0]).start()
        return carry

    lax.fori_loop(0, units // 128, down_step, 0)
    total_step(groups - 1)
    returned[e] = send_stage[0]

    def weight_step(i, carry):
        cut = pl.ds(pl.multiple_of(i * 256, 256), 256)
        both = lax.dot_general(
            toks[:, cut], d_both[...], DOWNWARD, preferred_element_type=f32
        ).astype(bf16)
        gate_stage[cut, :] = both[:, :units]
        up_stage[cut, :] = both[:, units:]
        pltpu.make_async_copy(gate_stage.at[cut], gate_out.at[cut], out_sem.at[1]).start()
        pltpu.make_async_copy(up_stage.at[cut], up_out.at[cut], out_sem.at[2]).start()
        return carry

    lax.fori_loop(0, model_width // 256, weight_step, 0)

    def close(k, carry):
        for a in range(2):
            to_pair(a, k, p).wait_send()
            to_mate(a, k, p, 0, own_columns).wait_send()
            to_mate(a, k, 1 - p, 1, own_columns).wait_send()
        core_copy(0, k).wait_send()
        core_copy(1, k).wait_send()
        pair_copy(k).wait_send()

        @pl.when(k > 0)
        def _():
            direct(0, k).wait_send()
            direct(1, k).wait_send()
            source = lax.rem(e + k, experts)
            remote(
                returned.at[source], returned.at[source], back_send.at[k], back_recv.at[k],
                (source, p, t),
            ).wait_recv()
            back_copy(k).wait_send()

        return carry

    lax.fori_loop(0, experts, close, 0)
    pltpu.make_async_copy(down_stage, down_out, out_sem.at[0]).wait()
    pltpu.make_async_copy(gate_stage, gate_out, out_sem.at[1]).wait()
    pltpu.make_async_copy(up_stage, up_out, out_sem.at[2]).wait()


def expert_rows(cap, ids, route_weights, moe_input, out_grad, gate_w, up_w, down_w):
    experts = lax.axis_size("ep")
    model_width, units = gate_w.shape
    width = model_width // lax.axis_size("tp")
    rows = experts * 2 * cap
    half = (experts, cap, width)
    vmem = pl.BlockSpec(memory_space=pltpu.VMEM)
    hbm = pl.BlockSpec(memory_space=pltpu.HBM)
    dma = pltpu.SemaphoreType.DMA
    wide, tall = (model_width, units), (units, model_width)
    kind, f32 = jnp.bfloat16, jnp.float32
    shape = jax.ShapeDtypeStruct
    group_rows = PER_GROUP * 2 * cap
    return pl.pallas_call(
        functools.partial(experts_kernel, experts, cap),
        out_shape=(shape(half, kind), shape(wide, kind), shape(wide, kind), shape(tall, kind)),
        in_specs=[vmem] * 4 + [hbm] * 3,
        out_specs=(vmem, hbm, hbm, hbm),
        scratch_shapes=[
            pltpu.VMEM((rows, model_width), kind),
            pltpu.VMEM((rows, model_width), kind),
            pltpu.VMEM((rows, units), kind),
            pltpu.VMEM((rows, 2 * units), kind),
            pltpu.VMEM((model_width, 2 * units), kind),
            pltpu.VMEM(tall, kind),
            pltpu.VMEM((group_rows, units), f32),
            pltpu.VMEM((group_rows, units), f32),
            pltpu.VMEM((rows, model_width), kind),
            pltpu.VMEM((experts, moe_input.shape[0]), jnp.int32),
            pltpu.VMEM(half, kind),
            pltpu.VMEM(half, kind),
            pltpu.VMEM((2,) + half, kind),
            pltpu.VMEM(half, kind),
            pltpu.VMEM(half, kind),
            pltpu.VMEM(half, kind),
            pltpu.VMEM(wide, kind),
            pltpu.VMEM(wide, kind),
            pltpu.VMEM(tall, kind),
            dma((3,)),
            dma((3,)),
            dma((2, experts)),
            dma((2, experts)),
            dma((2, experts)),
            dma((2, experts)),
            dma((2, 2, experts)),
            dma((2, 2, experts)),
            dma((2, experts)),
            dma((2, experts)),
            dma((experts,)),
            dma((experts,)),
            dma((experts,)),
            dma((experts,)),
        ],
        compiler_params=pltpu.CompilerParams(
            collective_id=0, has_side_effects=True, vmem_limit_bytes=60 * 1024 * 1024
        ),
        name="expert_rows",
    )(ids, route_weights, moe_input, out_grad, gate_w, up_w, down_w)


def attend_kernel(
    count, tp_count, rows, cap, ids, out_grad, returned, out_weight, queries, keys, values,
    log_decay, block_states,
    mid_columns, from_right, decay_dots, right_terms, grad_q, key_local, value_local, contrib_local,
    k_fade, fade_out,
    mid, mid_stage, early_stage, early_held, sum_stage, sum_held, result, dot_result, gathered,
    local_sem, mid_send, mid_recv, col_send, col_recv, pass_send, pass_recv,
    early_send, early_recv, sum_send, sum_recv, back_send, back_recv, dot_send, dot_recv,
    term_send, term_recv,
):
    me = sp_index()
    t = lax.axis_index("tp")
    tokens, channels = queries.shape
    heads = channels // DK
    blocks = tokens // BLK
    width = mid.shape[1] // tp_count
    share = count // tp_count
    f32, bf16 = jnp.float32, jnp.bfloat16

    def place(i, core):
        return (lax.div(i, 2), lax.rem(i, 2), core)

    barrier = pltpu.get_barrier_semaphore()
    for k in range(1, count):
        pl.semaphore_signal(
            barrier, inc=1, device_id=place(lax.rem(me + k, count), t), device_id_type=MESH
        )
    pl.semaphore_signal(barrier, inc=1, device_id=place(me, 1 - t), device_id_type=MESH)

    def dot(x, y, dims=(((1,), (0,)), ((), ()))):
        return lax.dot_general(
            x.astype(bf16), y.astype(bf16), dims, preferred_element_type=f32
        )

    def spread(src, dst, sends, recvs, k):
        dest = lax.rem(me + k, count)
        return pltpu.make_async_remote_copy(
            src_ref=src(dest), dst_ref=dst, send_sem=sends.at[k], recv_sem=recvs.at[k],
            device_id=place(dest, t), device_id_type=MESH,
        )

    def landed(ref, sends, recvs, k):
        source = lax.rem(me - k + count, count)
        pltpu.make_async_remote_copy(
            src_ref=ref.at[source], dst_ref=ref.at[source], send_sem=sends.at[k],
            recv_sem=recvs.at[k], device_id=place(source, t), device_id_type=MESH,
        ).wait_recv()

    row = lax.broadcasted_iota(jnp.int32, (tokens, tokens), 0)
    col = lax.broadcasted_iota(jnp.int32, (tokens, tokens), 1)
    earlier = (row >= col).astype(f32)
    decay = log_decay[...]
    position = lax.dot_general(
        earlier, decay, (((1,), (0,)), ((), ())), precision=PRECISE, preferred_element_type=f32
    )
    device_total = position[tokens - 1 :]
    fade = jnp.exp(device_total - position)
    k_all = keys[...].astype(f32)
    q_all = queries[...].astype(f32)
    v_all = values[...]
    faded = k_all * fade
    fade_out[...] = fade
    k_fade[...] = faded
    gain = jnp.transpose(jnp.broadcast_to(jnp.exp(device_total), (DV, channels)))

    for h in range(heads):
        ks, vs = slice(h * DK, (h + 1) * DK), slice(h * DV, (h + 1) * DV)
        reach = dot(faded[:, ks], v_all[:, vs], DOWNWARD)
        for j in range(DK // rows):
            cut = slice(j * rows, (j + 1) * rows)
            early_stage[h * (DK // rows) + j, 0] = reach[cut]
            early_stage[h * (DK // rows) + j, 1] = gain[h * DK + j * rows : h * DK + (j + 1) * rows]
    pl.semaphore_wait(barrier, count)
    early_held[me] = early_stage[me]
    for k in range(1, count):
        spread(lambda i: early_stage.at[i], early_held.at[me], early_send, early_recv, k).start()

    slot_count = returned.shape[0]
    expert_lane = lax.broadcasted_iota(jnp.int32, (tokens, slot_count // cap), 1)
    turned = [jnp.transpose(jnp.broadcast_to(ids[j : j + 1], (128, tokens))) for j in range(2)]
    first, second = expert_lane == turned[0][:, 0:1], expert_lane == turned[1][:, 0:1]
    rank = dot((row > col).astype(f32), (first | second).astype(f32)).astype(jnp.int32)
    spots = expert_lane * cap + rank
    slot_lane = lax.broadcasted_iota(jnp.int32, (tokens, slot_count), 1)
    first_slot = jnp.sum(jnp.where(first, spots, 0), axis=1, keepdims=True)
    second_slot = jnp.sum(jnp.where(second, spots, 0), axis=1, keepdims=True)
    pick = (slot_lane == first_slot) | (slot_lane == second_slot)
    own_columns = pl.ds(pl.multiple_of(t * width, 128), width)
    core_columns = pl.ds(pl.multiple_of((1 - t) * width, 128), width)
    moe = dot(pick.astype(f32), returned[...])
    mid_half = (out_grad[:, own_columns].astype(f32) + moe).astype(bf16)
    mid[:, own_columns] = mid_half

    def to_core(columns):
        return pltpu.make_async_remote_copy(
            src_ref=mid.at[:, columns], dst_ref=mid.at[:, columns], send_sem=mid_send,
            recv_sem=mid_recv, device_id=place(me, 1 - t), device_id_type=MESH,
        )

    to_core(own_columns).start()
    piece = width // share
    for j in range(share):
        mid_stage[j] = mid_half[:, j * piece : (j + 1) * piece]

    cumul = [position[:BLK]]
    for n in range(1, blocks):
        cumul.append(position[n * BLK : (n + 1) * BLK] - position[n * BLK - 1 : n * BLK])
    growth = [jnp.exp(c) for c in cumul]
    shrink = [jnp.exp(-c) for c in cumul]
    to_end = [jnp.exp(c[BLK - 1 :] - c) for c in cumul]
    span = [slice(n * BLK, (n + 1) * BLK) for n in range(blocks)]
    q_grow = [(q_all[span[n]] * growth[n]).astype(bf16) for n in range(blocks)]
    k_shrink = [(k_all[span[n]] * shrink[n]).astype(bf16) for n in range(blocks)]
    k_end = [(k_all[span[n]] * to_end[n]).astype(bf16) for n in range(blocks)]
    q_long = (q_all * jnp.exp(position)).astype(bf16)

    to_core(core_columns).wait_recv()
    o_all = dot(mid[...], out_weight[...], ACROSS).astype(bf16)
    for h in range(heads):
        ks, vs = slice(h * DK, (h + 1) * DK), slice(h * DV, (h + 1) * DV)
        summed = dot(q_long[:, ks], o_all[:, vs], DOWNWARD)
        for j in range(DK // rows):
            sum_stage[h * (DK // rows) + j] = summed[j * rows : (j + 1) * rows]
    sum_held[me] = sum_stage[me]
    for k in range(1, count):
        spread(lambda i: sum_stage.at[i], sum_held.at[me], sum_send, sum_recv, k).start()

    def own_share(c):
        return lax.div(c, share) == t

    def column_copy(j):
        dest = t * share + lax.rem(me + j, share)
        return pltpu.make_async_remote_copy(
            src_ref=mid_stage.at[lax.rem(me + j, share)], dst_ref=mid_columns.at[me],
            send_sem=col_send.at[j], recv_sem=col_recv.at[lax.rem(dest - me + count, count)],
            device_id=place(dest, t), device_id_type=MESH,
        )

    def column_self(c):
        return pltpu.make_async_copy(
            mid_stage.at[lax.rem(c, share)], mid_columns.at[c], local_sem
        )

    for j in range(share):

        @pl.when(t * share + lax.rem(me + j, share) != me)
        def _():
            column_copy(j).start()

    @pl.when(own_share(me))
    def _():
        column_self(me).start()

    lane_causal = row[:BLK, :BLK] >= col[:BLK, :BLK]
    lane_causal_t = row[:BLK, :BLK] <= col[:BLK, :BLK]
    for n in range(blocks - 1, -1, -1):
        for h in range(heads):
            ks, vs = slice(h * DK, (h + 1) * DK), slice(h * DV, (h + 1) * DV)
            o, v = o_all[span[n], vs], v_all[span[n], vs]
            qg, kk = q_grow[n][:, ks], k_shrink[n][:, ks]
            state_in = block_states[n, h].astype(bf16)
            scores = jnp.where(lane_causal, dot(o, v, ACROSS), 0.0)
            scores_t = jnp.where(lane_causal_t, dot(v, o, ACROSS), 0.0)
            mutual_t = jnp.where(lane_causal_t, dot(kk, qg, ACROSS), 0.0)
            gq = growth[n][:, ks] * (dot(o, state_in, ACROSS) + dot(scores, kk))
            gk = shrink[n][:, ks] * dot(scores_t, qg)
            gv = dot(mutual_t, o)
            if n < blocks - 1:
                later = slice((n + 1) * BLK, tokens)
                end = position[(n + 1) * BLK - 1 : (n + 1) * BLK, ks]
                carried = dot(
                    q_all[later, ks] * jnp.exp(position[later, ks] - end), o_all[later, vs], DOWNWARD
                )
                gk = gk + to_end[n][:, ks] * dot(v, carried, ACROSS)
                gv = gv + dot(k_end[n][:, ks], carried)
            grad_q[span[n], ks] = gq
            key_local[span[n], ks] = gk
            value_local[span[n], vs] = gv
    contrib = q_all * grad_q[...] - k_all * key_local[...]
    contrib_local[...] = contrib
    gathered[me] = jnp.sum(contrib, axis=0, keepdims=True)
    for k in range(1, count):
        spread(lambda i: gathered.at[me], gathered.at[me], term_send, term_recv, k).start()

    for k in range(1, count):
        landed(early_held, early_send, early_recv, k)
    for k in range(1, count):
        landed(sum_held, sum_send, sum_recv, k)
    total = jnp.zeros((rows, DV), f32)
    dots = jnp.zeros((rows, DV), f32)
    for i in range(count - 1, -1, -1):
        result[i] = total
        dot_result[i] = dots
        reach_dot = jnp.sum(early_held[i, 0] * total, axis=1, keepdims=True)
        dots = dots + jnp.broadcast_to(reach_dot, (rows, DV))
        total = early_held[i, 1] * total + sum_held[i]
    from_right[me] = result[me]
    decay_dots[me] = dot_result[me]
    for k in range(1, count):
        spread(lambda i: result.at[i], from_right.at[me], back_send, back_recv, k).start()
    for k in range(1, count):
        spread(lambda i: dot_result.at[i], decay_dots.at[me], dot_send, dot_recv, k).start()

    def pass_copy(c, index):
        return pltpu.make_async_remote_copy(
            src_ref=mid_columns.at[c], dst_ref=mid_columns.at[c], send_sem=pass_send.at[index],
            recv_sem=pass_recv.at[index], device_id=place(me, 1 - t), device_id_type=MESH,
        )

    @pl.when(own_share(me))
    def _():
        column_self(me).wait()
        pass_copy(me, 0).start()
        for k in range(1, count):
            landed(mid_columns, pass_send, col_recv, k)
            pass_copy(lax.rem(me - k + count, count), k).start()

    @pl.when(jnp.logical_not(own_share(me)))
    def _():
        for k in range(count):
            pass_copy(lax.rem(me - k + count, count), k).wait_recv()

    for k in range(1, count):
        landed(gathered, term_send, term_recv, k)
    summed_terms = jnp.zeros((1, channels), f32)
    for i in range(count):
        summed_terms += jnp.where(i > me, gathered[i], 0.0)
    right_terms[...] = summed_terms
    for k in range(1, count):
        landed(from_right, back_send, back_recv, k)
        landed(decay_dots, dot_send, dot_recv, k)
    to_core(own_columns).wait_send()
    for j in range(share):

        @pl.when(t * share + lax.rem(me + j, share) != me)
        def _():
            column_copy(j).wait_send()

    @pl.when(own_share(me))
    def _():
        for k in range(count):
            pass_copy(lax.rem(me - k + count, count), k).wait_send()

    for k in range(1, count):
        spread(lambda i: early_stage.at[i], early_held.at[me], early_send, early_recv, k).wait_send()
        spread(lambda i: sum_stage.at[i], sum_held.at[me], sum_send, sum_recv, k).wait_send()
        spread(lambda i: result.at[i], from_right.at[me], back_send, back_recv, k).wait_send()
        spread(lambda i: dot_result.at[i], decay_dots.at[me], dot_send, dot_recv, k).wait_send()
        spread(lambda i: gathered.at[me], gathered.at[me], term_send, term_recv, k).wait_send()


def attend(cap, ids, out_grad, returned, out_weight, queries, keys, values, log_decay, block_states):
    count = sp_size()
    tp_count = lax.axis_size("tp")
    tokens, channels = queries.shape
    model_width = out_grad.shape[1]
    heads = channels // DK
    rows = channels // count
    share = count // tp_count
    piece = model_width // count
    f32, bf16 = jnp.float32, jnp.bfloat16
    vmem = pl.BlockSpec(memory_space=pltpu.VMEM)
    dma = pltpu.SemaphoreType.DMA
    shape = jax.ShapeDtypeStruct
    wide = shape((tokens, channels), f32)
    return pl.pallas_call(
        functools.partial(attend_kernel, count, tp_count, rows, cap),
        out_shape=(
            shape((count, tokens, piece), bf16),
            shape((count, rows, DV), f32),
            shape((count, rows, DV), f32),
            shape((1, channels), f32),
            wide,
            wide,
            shape((tokens, heads * DV), f32),
            wide,
            wide,
            wide,
        ),
        in_specs=[vmem] * 9,
        out_specs=(vmem,) * 10,
        scratch_shapes=[
            pltpu.VMEM((tokens, model_width), bf16),
            pltpu.VMEM((share, tokens, piece), bf16),
            pltpu.VMEM((count, 2, rows, DV), f32),
            pltpu.VMEM((count, 2, rows, DV), f32),
            pltpu.VMEM((count, rows, DV), f32),
            pltpu.VMEM((count, rows, DV), f32),
            pltpu.VMEM((count, rows, DV), f32),
            pltpu.VMEM((count, rows, DV), f32),
            pltpu.VMEM((count, 1, channels), f32),
            dma,
            dma,
            dma,
            dma((share,)),
            dma((count,)),
            dma((count,)),
            dma((count,)),
            dma((count,)),
            dma((count,)),
            dma((count,)),
            dma((count,)),
            dma((count,)),
            dma((count,)),
            dma((count,)),
            dma((count,)),
            dma((count,)),
            dma((count,)),
        ],
        compiler_params=pltpu.CompilerParams(
            collective_id=1, has_side_effects=True, vmem_limit_bytes=60 * 1024 * 1024
        ),
        name="attend",
    )(ids, out_grad, returned, out_weight, queries, keys, values, log_decay, block_states)


def finish_kernel(
    chunks, mixer, mid_columns, from_right, decay_dots, right_terms, query_local, key_local,
    value_local, contrib_local, k_fade, fade_out, values, weight_a, weight_b, weight_c,
    grad_q, grad_k, grad_v, grad_decay, grad_out, out_a, out_b, out_c,
    hold_a, hold_b, hold_c, in_sem, out_sem,
):
    f32, bf16 = jnp.float32, jnp.bfloat16
    trios = ((weight_a, hold_a, out_a), (weight_b, hold_b, out_b), (weight_c, hold_c, out_c))

    def moves(a, j):
        source, hold, target = trios[a]
        size = source.shape[0] // chunks
        cut = pl.ds(j * size, size)
        return (
            pltpu.make_async_copy(source.at[cut], hold.at[cut], in_sem.at[a, j]),
            pltpu.make_async_copy(hold.at[cut], target.at[cut], out_sem.at[a, j]),
        )

    steps = [(a, j) for a in range(3) for j in range(chunks)]
    for a, j in steps:
        moves(a, j)[0].start()

    def dot(x, y, dims=(((1,), (0,)), ((), ()))):
        return lax.dot_general(
            x.astype(bf16), y.astype(bf16), dims, preferred_element_type=f32
        )

    def forward(group):
        for a, j in group:
            moves(a, j)[0].wait()
            moves(a, j)[1].start()

    tokens, channels = key_local.shape
    heads = channels // DK
    grad_q[...] = query_local[...].astype(bf16)
    forward(steps[:chunks])
    key_parts = []
    for h in range(heads):
        ks, vs = slice(h * DK, (h + 1) * DK), slice(h * DV, (h + 1) * DV)
        carried = from_right[h].astype(bf16)
        key_parts.append(dot(values[:, vs], carried, ACROSS))
        grad_v[:, vs] = (value_local[:, vs] + dot(k_fade[:, ks], carried)).astype(bf16)
    key_part = jnp.concatenate(key_parts, axis=1)
    grad_k[...] = (key_local[...] + fade_out[...] * key_part).astype(bf16)
    contrib = contrib_local[...] - k_fade[...] * key_part
    forward(steps[chunks : 2 * chunks])
    row = lax.broadcasted_iota(jnp.int32, (tokens, tokens), 0)
    col = lax.broadcasted_iota(jnp.int32, (tokens, tokens), 1)
    later = (col >= row).astype(f32)
    groups = []
    spot = lax.broadcasted_iota(jnp.int32, (128, 128), 0)
    lane = lax.broadcasted_iota(jnp.int32, (128, 128), 1)
    for g in range(channels // 128):
        picked = jnp.where(spot == lane, decay_dots[g * 128 : (g + 1) * 128], 0.0)
        groups.append(jnp.sum(picked, axis=0, keepdims=True))
    right = right_terms[...] - jnp.concatenate(groups, axis=1)
    grad_decay[...] = right + lax.dot_general(
        later, contrib, (((1,), (0,)), ((), ())), precision=PRECISE, preferred_element_type=f32
    )
    grad_out[...] = dot(mixer[...], mid_columns[...], DOWNWARD)
    forward(steps[2 * chunks :])
    for a, j in steps:
        moves(a, j)[1].wait()


def finish(mixer, local, values, weights):
    mid_columns, from_right, decay_dots, right_terms, *rest = local
    tokens, channels = rest[1].shape
    heads = channels // DK
    mid_columns = mid_columns.reshape(mixer.shape[0], -1)
    from_right = from_right.reshape(heads, DK, DV)
    decay_dots = decay_dots.reshape(channels, DV)
    vmem = pl.BlockSpec(memory_space=pltpu.VMEM)
    hbm = pl.BlockSpec(memory_space=pltpu.HBM)
    dma = pltpu.SemaphoreType.DMA
    shape = jax.ShapeDtypeStruct
    f32, bf16 = jnp.float32, jnp.bfloat16
    chunks = 4
    return pl.pallas_call(
        functools.partial(finish_kernel, chunks),
        out_shape=(
            shape((tokens, channels), bf16),
            shape((tokens, channels), bf16),
            shape((tokens, heads * DV), bf16),
            shape((tokens, channels), f32),
            shape((mixer.shape[1], mid_columns.shape[1]), f32),
            *(shape(w.shape, w.dtype) for w in weights),
        ),
        in_specs=[vmem] * 12 + [hbm] * 3,
        out_specs=(vmem,) * 5 + (hbm,) * 3,
        scratch_shapes=[pltpu.VMEM(w.shape, w.dtype) for w in weights]
        + [dma((3, chunks)), dma((3, chunks))],
        compiler_params=pltpu.CompilerParams(vmem_limit_bytes=60 * 1024 * 1024),
        name="finish",
    )(mixer, mid_columns, from_right, decay_dots, right_terms, *rest, values, *weights)


def body(
    moe_input,
    out_grad,
    route_ids,
    route_weights,
    gate_w,
    up_w,
    down_w,
    mixer_out,
    out_weight,
    queries,
    keys,
    values,
    log_decay,
    block_states,
):
    experts = lax.axis_size("ep")
    cap = -(-3 * moe_input.shape[0] // experts // 16) * 16
    returned, *weights = expert_rows(
        cap, route_ids.T, route_weights.T, moe_input, out_grad, gate_w[0], up_w[0], down_w[0]
    )
    mixer_all = lax.all_gather(mixer_out, SP, axis=0, tiled=True)
    local = attend(
        cap, route_ids.T, out_grad, returned.reshape(experts * cap, -1), out_weight, queries, keys,
        values, log_decay, block_states,
    )
    grad_q, grad_k, grad_v, grad_decay, grad_out_weight, grad_gate, grad_up, grad_down = finish(
        mixer_all, local, values, weights
    )
    return (
        grad_q,
        grad_k,
        grad_v,
        grad_decay,
        grad_out_weight,
        grad_gate[None],
        grad_up[None],
        grad_down[None],
    )


def solution(mesh):
    sp_count, tp_count = mesh.devices.shape
    mesh = Mesh(mesh.devices.reshape(sp_count // 2, 2, tp_count), ("ep", "pair", "tp"))
    placed = (
        P(SP, None),
        P(SP, None),
        P(SP, None),
        P(SP, None),
        P(SP, None, "tp"),
        P(SP, None, "tp"),
        P(SP, "tp", None),
        P(SP, "tp"),
        P("tp", None),
        P(SP, "tp"),
        P(SP, "tp"),
        P(SP, "tp"),
        P(SP, "tp"),
        P(SP, "tp", None, None),
    )
    return jax.shard_map(
        body,
        mesh=mesh,
        in_specs=placed,
        out_specs=(
            P(SP, "tp"),
            P(SP, "tp"),
            P(SP, "tp"),
            P(SP, "tp"),
            P("tp", SP),
            P(SP, None, "tp"),
            P(SP, None, "tp"),
            P(SP, "tp", None),
        ),
        check_vma=False,
    )
```

time: 243 us -> 170 us (0.70)
  matrix products: 48.2 us -> 0 us
  local copies, waits for them, and re-layouts: 34.4 us -> 0 us
  Pallas kernels: 122 us -> 155 us
  starting transfers between devices: 10 us -> 0.04 us
  other arithmetic: 9.75 us -> 0 us
    dot_general x30 -> x0, matrix products: 46.9 us -> none  [the longest x1 6.53 us: body(): jnp.dot(arrived_tokens, gate_mat, preferred_element_type=jnp.float32)]
    pallas_call x3, Pallas kernels: 122 us -> 155 us  [the longest x1 114 us: expert_rows(): pl.pallas_call(functools.partial(experts_kernel, experts, cap), out_shape...]
    unnamed x51 -> x0, local copies, waits for them, and re-layouts: 12.2 us -> none
    all_to_all x1 -> x0, starting transfers between devices: 9.96 us -> none  [body(): lax.all_to_all(grad_mid, SP, split_axis=1, concat_axis=0, tiled=True)]
    reshape x8 -> x0, local copies, waits for them, and re-layouts: 5.44 us -> none  [the longest x6 4.58 us: shaped(): return array.astype(jnp.float32).reshape(blocks, BLK, heads_local, depth)]
    another operation x8 -> x0, other arithmetic: 4.52 us -> none  [the longest x2 1.96 us: block_back(): cumul = jnp.cumsum(decay_block, axis=0)]
    dynamic_slice x8 -> x0, local copies, waits for them, and re-layouts: 4.36 us -> none  [body(): lax.scan(block_back, zero_state, inputs, reverse=True)]
    mul x4 -> x0, local copies, waits for them, and re-layouts: 3.54 us -> none  [the longest x3 3.41 us: body(): route_weights[:, :, None] * source_grads[:, None, :].astype(jnp.float32)]
  transfers between devices with their start and end apart: 2 -> 1, of which waited for: 0 -> 0; matrix products, arithmetic and copies ran while one was open for 17% -> 0% of each run, Pallas kernels for 12% -> 85%
where the time goes in v1:
time: 170 us; the launch traced here: 169 us
  Pallas kernels  155 us (91%)
  between operations  14.1 us (8%)
    pallas_call x1, Pallas kernels, expert_rows(): pl.pallas_call(functools.partial(experts_kernel, experts, cap), out_shape...  114 us
    pallas_call x1, Pallas kernels, attend(): pl.pallas_call(functools.partial(attend_kernel, count, tp_count, rows, ca...  29.9 us
    pallas_call x1, Pallas kernels, finish(): pl.pallas_call(functools.partial(finish_kernel, chunks), out_shape=(shape...  10.8 us
  transfers between devices with their start and end apart: 1, of which 0 were waited for; matrix products, arithmetic and copies ran while one was open for 0% of the time, Pallas kernels for 85%

profile of v1, /device:TPU:0, one launch (start us, length us, event | category | flops | bytes accessed | tf_op | source)
XLA Modules:
  0.0 169.4 jit_solution(2710801620823026275)
XLA Ops:
  7.2 0.0 all-gather.2.cloned.1.call-start
  7.2 0.7 all-gather.2.cloned.1.call-update
  7.9 113.8 %expert_rows.1 = (bf16[8,48,1024]{2,1,0:T(8,128)(2,1)}, bf16[2048,896]{1,0:T(8,128)(2,1)}, bf16[2048,896]{1,0:T(8,128)(2,1)}, bf16[896,2048]{1,0:T(8,128)(2,1)}) custom-call(s32[2,128]{1,0:T(2,128)} %bitcast.19, f32[2,128]{1,0:T(2,128)} %bitcast.21, bf16[128,2048]{1,0:T(8,128)(2,1)} %moe_input.1, bf16[128,2048]{1,0:T(8,128)(2,1)} %out_grad.3, ...), custom_call_target="tpu_custom_call" | custom-call | tf_op jit(solution)/shard_map/expert_rows/pallas_call | solution.py:326
  121.7 29.9 %attend.1 = (bf16[16,128,128]{2,1,0:T(8,128)(2,1)}, f32[16,16,128]{2,1,0:T(8,128)}, f32[16,16,128]{2,1,0:T(8,128)}, f32[1,256]{1,0:T(1,128)}, f32[128,256]{1,0:T...) custom-call(s32[2,128]{1,0:T(2,128)} %bitcast.20, ...), custom_call_target="tpu_custom_call" | custom-call | tf_op jit(solution)/shard_map/attend/pallas_call | solution.py:638
  151.7 0.0 all-gather.2.cloned.1.call-done.mixer
  151.7 10.8 %finish.1 = (bf16[128,256]{1,0:T(8,128)(2,1)}, bf16[128,256]{1,0:T(8,128)(2,1)}, bf16[128,512]{1,0:T(8,128)(2,1)}, f32[128,256]{1,0:T(8,128)}, f32[512,128]{1,0:...) custom-call(bf16[2048,512]{1,0:T(8,128)(2,1)} %all-gather.2.cloned.1.call-done.mixer, ...), custom_call_target="tpu_custom_call" | custom-call | tf_op jit(solution)/shard_map/finish/pallas_call | solution.py:767
Async XLA Ops:
  7.2 144.5 %all-gather.2.cloned.1.call-start = ((), (), s32[]{:S(2)}) async-start(), calls=%async_computation | async-start | bytes 2228224 | tf_op jit(solution)/shard_map/all_gather | solution.py:807
Sparse Core Ops, SparseCore 0:
  10.7 82.6 all-gather.1

commit v2 on v1

v2 whole, which is shorter than its diff:
```python
import functools

import jax
import jax.numpy as jnp
from jax import lax
from jax.experimental import pallas as pl
from jax.experimental.pallas import tpu as pltpu
from jax.sharding import Mesh, PartitionSpec as P

MESH = pl.DeviceIdType.MESH
SP = ("ep", "pair")

DK = 64
DV = 128
BLK = 64
PER_GROUP = 2


PRECISE = lax.Precision.HIGHEST
ACROSS = (((1,), (1,)), ((), ()))
DOWNWARD = (((0,), (0,)), ((), ()))
PLAIN = (((1,), (0,)), ((), ()))


def sp_size():
    return lax.axis_size("ep") * lax.axis_size("pair")


def sp_index():
    return lax.axis_index("ep") * lax.axis_size("pair") + lax.axis_index("pair")


def experts_kernel(
    experts, cap, ids, route_weights, moe_input, out_grad, gate_w, up_w, down_w,
    mixer_hbm, out_weight_hbm, queries_hbm, keys_hbm, values_hbm, log_decay_hbm, block_states_hbm,
    gate_out, up_out, down_out, grad_out, from_right, decay_dots, right_terms, grad_q, key_local,
    value_local, contrib_local, k_fade, fade_out,
    out_weight, queries, keys, values, log_decay, block_states, mixers, returned, position_ref,
    mid, mid_stage, mid_columns, early_stage, early_held, sum_stage, sum_held, result, dot_result,
    gathered, near_part, near_held,
    toks, grads, hidden, d_both, gate_up, down, silu_part, slope_part, parts, rank, tok_send,
    grad_send, core_held, pair_stage, pair_held, send_stage, gate_stage, up_stage, down_stage,
    weight_sem, out_sem, direct_send, direct_recv, pass_send, pass_recv, mate_send, mate_recv,
    core_send, core_recv, pair_send, pair_recv, back_send, back_recv,
    load_sem, mixer_send, mixer_recv, side_send, side_recv, mid_send, mid_recv, col_send, col_recv,
    cross_send, cross_recv, near_send, near_recv, early_send, early_recv, sum_send, sum_recv,
    right_send, right_recv, dot_send, dot_recv, term_send, term_recv,
):
    e, p, t = lax.axis_index("ep"), lax.axis_index("pair"), lax.axis_index("tp")
    f32, bf16 = jnp.float32, jnp.bfloat16
    tokens, model_width = moe_input.shape
    width = model_width // 2
    units = hidden.shape[1]
    group_rows = PER_GROUP * 2 * cap
    groups = experts // PER_GROUP
    pair_id, mate_id = (e, 1 - p, t), (e, p, 1 - t)
    barrier = pltpu.get_barrier_semaphore()
    me = e * 2 + p
    count = experts * 2
    half_experts = experts // 2
    low, high = lax.rem(e, 2), lax.div(e, 2)
    here = high * 2 + p

    def place(i):
        return (lax.div(i, 2), lax.rem(i, 2), t)

    for k in range(1, count):
        pl.semaphore_signal(
            barrier, inc=1, device_id=place(lax.rem(me + k, count)), device_id_type=MESH
        )
    pl.semaphore_signal(barrier, inc=1, device_id=mate_id, device_id_type=MESH)

    def flip(k):
        total, bit = 0, 1
        while bit < experts:
            other = k // bit if isinstance(k, int) else lax.div(k, bit)
            total = total + bit * lax.rem(lax.div(e, bit) + other, 2)
            bit *= 2
        return total

    own_mixer = pltpu.make_async_copy(mixer_hbm, mixers.at[here], load_sem.at[6])
    late = [
        pltpu.make_async_copy(src, dst, load_sem.at[i])
        for i, (src, dst) in enumerate(
            (
                (log_decay_hbm, log_decay),
                (keys_hbm, keys),
                (values_hbm, values),
                (queries_hbm, queries),
                (out_weight_hbm, out_weight),
                (block_states_hbm, block_states),
            )
        )
    ]
    loads = (
        pltpu.make_async_copy(gate_w, gate_up.at[:, pl.ds(0, units)], weight_sem.at[0]),
        pltpu.make_async_copy(up_w, gate_up.at[:, pl.ds(units, units)], weight_sem.at[1]),
        pltpu.make_async_copy(down_w, down, weight_sem.at[2]),
    )
    for load in late[:3] + list(loads) + late[3:] + [own_mixer]:
        load.start()
    own_columns = pl.ds(pl.multiple_of(t * width, 128), width)
    core_columns = pl.ds(pl.multiple_of((1 - t) * width, 128), width)
    arrived = (toks, grads)
    sends = (tok_send, grad_send)

    def block(k, side):
        return pl.ds(pl.multiple_of((k * 2 + side) * cap, cap), cap)

    def remote(src, dst, send, recv, device):
        return pltpu.make_async_remote_copy(
            src_ref=src, dst_ref=dst, send_sem=send, recv_sem=recv, device_id=device,
            device_id_type=MESH,
        )

    def direct(a, k):
        return remote(
            sends[a].at[k], arrived[a].at[block(k, p), own_columns], direct_send.at[a, k],
            direct_recv.at[a, k], (flip(k), p, t),
        )

    def to_pair(a, k, side):
        place = arrived[a].at[block(k, side), own_columns]
        return remote(place, place, pass_send.at[a, k], pass_recv.at[a, k], pair_id)

    def to_mate(a, k, side, which, columns):
        place = arrived[a].at[block(k, side), columns]
        return remote(place, place, mate_send.at[a, which, k], mate_recv.at[a, which, k], mate_id)

    first_id, second_id = ids[0:1], ids[1:2]
    first_w, second_w = route_weights[0:1], route_weights[1:2]
    expert_row = lax.broadcasted_iota(jnp.int32, (experts, tokens), 0)
    member = (expert_row == first_id) | (expert_row == second_id)
    row = lax.broadcasted_iota(jnp.int32, (tokens, tokens), 0)
    col = lax.broadcasted_iota(jnp.int32, (tokens, tokens), 1)
    before = (row < col).astype(bf16)
    earlier = lax.dot_general(
        member.astype(f32).astype(bf16), before, PLAIN, preferred_element_type=f32
    )
    rank[...] = jnp.where(member, earlier.astype(jnp.int32), -1)
    spot = lax.broadcasted_iota(jnp.int32, (cap, tokens), 0)

    def rows_for(dest):
        pick = spot == rank[pl.ds(dest, 1)]
        weight = jnp.where(first_id == dest, first_w, second_w)
        scale = jnp.sum(jnp.where(pick, weight, 0.0), axis=1, keepdims=True)
        chosen = pick.astype(f32).astype(bf16)
        tok = lax.dot_general(chosen, moe_input[:, own_columns], PLAIN, preferred_element_type=f32)
        grad = lax.dot_general(chosen, out_grad[:, own_columns], PLAIN, preferred_element_type=f32)
        return tok.astype(bf16), (scale * grad).astype(bf16)

    own_tok, own_grad = rows_for(e)
    toks[block(0, p), own_columns] = own_tok
    grads[block(0, p), own_columns] = own_grad
    pl.semaphore_wait(barrier, count)
    for a in range(2):
        to_pair(a, 0, p).start()
        to_mate(a, 0, p, 0, own_columns).start()

    def send_step(k, carry):
        tok, grad = rows_for(flip(k))
        tok_send[k] = tok
        grad_send[k] = grad
        direct(0, k).start()
        direct(1, k).start()
        return carry

    lax.fori_loop(1, experts, send_step, 0)

    def mixer_copy(k):
        dest = lax.rem(high + k, half_experts) * 2 + low
        return remote(
            mixer_hbm, mixers.at[here], mixer_send.at[k], mixer_recv.at[k], (dest, p, t)
        )

    def mixer_place(k, side):
        return mixers.at[lax.rem(high - k + half_experts, half_experts) * 2 + side]

    def mixer_landed(k):
        spot = mixer_place(k, p)
        remote(spot, spot, mixer_send.at[k], mixer_recv.at[k], pair_id).wait_recv()

    def mixer_side(k, side):
        spot = mixer_place(k, side)
        return remote(spot, spot, side_send.at[k], side_recv.at[k], pair_id)

    for k in range(1, half_experts):
        mixer_copy(k).start()

    channels = queries.shape[1]
    heads = channels // DK
    blocks = tokens // BLK
    rows = channels // count
    per_head = DK // rows

    def dot(x, y, dims=PLAIN):
        return lax.dot_general(
            x.astype(bf16), y.astype(bf16), dims, preferred_element_type=f32
        )

    def spread(src, dst, sends, recvs, k):
        dest = lax.rem(me + k, count)
        return remote(src(dest), dst, sends.at[k], recvs.at[k], place(dest))

    def landed(ref, sends, recvs, k):
        source = lax.rem(me - k + count, count)
        remote(ref.at[source], ref.at[source], sends.at[k], recvs.at[k], place(source)).wait_recv()

    def early_copy(k):
        return spread(lambda i: early_stage.at[i], early_held.at[me], early_send, early_recv, k)

    for load in late[:3]:
        load.wait()
    position_ref[...] = lax.dot_general(
        (row >= col).astype(f32), log_decay[...], PLAIN, precision=PRECISE,
        preferred_element_type=f32,
    )
    device_total = position_ref[tokens - 1 :]
    fade = jnp.exp(device_total - position_ref[...])
    faded = keys[...].astype(f32) * fade
    fade_out[...] = fade
    k_fade[...] = faded
    gain = jnp.transpose(jnp.broadcast_to(jnp.exp(device_total), (DV, channels)))
    for h in range(heads):
        ks, vs = slice(h * DK, (h + 1) * DK), slice(h * DV, (h + 1) * DV)
        reach = dot(faded[:, ks], values[:, vs], DOWNWARD)
        for j in range(per_head):
            early_stage[h * per_head + j, 0] = reach[j * rows : (j + 1) * rows]
            early_stage[h * per_head + j, 1] = gain[h * DK + j * rows : h * DK + (j + 1) * rows]
    early_held[me] = early_stage[me]
    for k in range(1, count):
        early_copy(k).start()
    for load in loads:
        load.wait()

    def from_direct(a, k):
        @pl.when(k > 0)
        def _():
            direct(a, k).wait_recv()
            to_pair(a, k, p).start()
            to_mate(a, k, p, 0, own_columns).start()

    def from_pair(a, k):
        to_pair(a, k, 1 - p).wait_recv()
        to_mate(a, k, 1 - p, 1, own_columns).start()

    def from_mate(a, k):
        to_mate(a, k, p, 0, core_columns).wait_recv()
        to_mate(a, k, 1 - p, 1, core_columns).wait_recv()

    def core_copy(which, k):
        side = 1 - p if which == 0 else p
        return remote(
            parts.at[block(k, side), core_columns], core_held.at[which, k],
            core_send.at[which, k], core_recv.at[which, k], mate_id,
        )

    def pair_copy(k):
        return remote(
            pair_stage.at[k], pair_held.at[k], pair_send.at[k], pair_recv.at[k], pair_id
        )

    def back_copy(k):
        return remote(
            send_stage.at[k], returned.at[pl.ds(pl.multiple_of(e * cap, cap), cap)], back_send.at[k], back_recv.at[k], (flip(k), p, t)
        )

    def half_of(which, k):
        side = 1 - p if which == 0 else p
        mine = parts[block(k, side), own_columns].astype(f32)
        return (mine + core_held[which, k].astype(f32)).astype(bf16)

    def members(g):
        return [g * PER_GROUP + j for j in range(PER_GROUP)]

    def half_step(g):
        for k in members(g):
            core_copy(0, k).wait_recv()
            pair_stage[k] = half_of(0, k)
            pair_copy(k).start()

    def total_step(g):
        for k in members(g):
            core_copy(1, k).wait_recv()
            pair_copy(k).wait_recv()
            total = half_of(1, k).astype(f32) + pair_held[k].astype(f32)
            send_stage[k] = total.astype(bf16)

            @pl.when(k > 0)
            def _():
                back_copy(k).start()

    def group_step(g, carry):
        now, last = members(g), members(g - 1)
        rows = pl.ds(pl.multiple_of((g - 1) * group_rows, group_rows), group_rows)
        coming, behind = g < groups, g > 0

        @pl.when(coming)
        def _():
            for k in now:
                from_direct(0, k)

        @pl.when(behind)
        def _():
            for k in last:
                from_mate(0, k)
            gate_pre = lax.dot_general(
                toks[rows], gate_up[:, :units], PLAIN, preferred_element_type=f32
            )
            gate = jax.nn.sigmoid(gate_pre)
            silu_part[...] = gate_pre * gate
            slope_part[...] = gate * (1.0 + gate_pre * (1.0 - gate))

        @pl.when(coming)
        def _():
            for k in now:
                from_direct(1, k)
                from_pair(0, k)

        @pl.when(behind)
        def _():
            up_pre = lax.dot_general(
                toks[rows], gate_up[:, units:], PLAIN, preferred_element_type=f32
            )
            hidden[rows] = (silu_part[...] * up_pre).astype(bf16)
            slope_part[...] = slope_part[...] * up_pre
            for k in last:
                from_mate(1, k)

        @pl.when(coming)
        def _():
            for k in now:
                from_pair(1, k)

        @pl.when(behind)
        def _():
            d_hidden = lax.dot_general(grads[rows], down[...], ACROSS, preferred_element_type=f32)
            d_both[rows, :units] = (d_hidden * slope_part[...]).astype(bf16)
            d_both[rows, units:] = (d_hidden * silu_part[...]).astype(bf16)
            parts[rows, core_columns] = lax.dot_general(
                d_both[rows], gate_up[core_columns], ACROSS, preferred_element_type=f32
            ).astype(bf16)
            for k in last:
                core_copy(0, k).start()
                core_copy(1, k).start()

        @pl.when(g > 1)
        def _():
            total_step(g - 2)

        @pl.when(behind)
        def _():
            parts[rows, own_columns] = lax.dot_general(
                d_both[rows], gate_up[own_columns], ACROSS, preferred_element_type=f32
            ).astype(bf16)
            half_step(g - 1)

        return carry

    lax.fori_loop(0, groups + 1, group_step, 0)

    def down_step(i, carry):
        cut = pl.ds(pl.multiple_of(i * 128, 128), 128)
        down_stage[cut, :] = lax.dot_general(
            hidden[:, cut], grads[...], DOWNWARD, preferred_element_type=f32
        ).astype(bf16)
        pltpu.make_async_copy(down_stage.at[cut], down_out.at[cut], out_sem.at[0]).start()
        return carry

    def weight_step(i, carry):
        cut = pl.ds(pl.multiple_of(i * 256, 256), 256)
        both = lax.dot_general(
            toks[:, cut], d_both[...], DOWNWARD, preferred_element_type=f32
        ).astype(bf16)
        gate_stage[cut, :] = both[:, :units]
        up_stage[cut, :] = both[:, units:]
        pltpu.make_async_copy(gate_stage.at[cut], gate_out.at[cut], out_sem.at[1]).start()
        pltpu.make_async_copy(up_stage.at[cut], up_out.at[cut], out_sem.at[2]).start()
        return carry

    weight_steps = model_width // 256
    first_cut, second_cut = weight_steps // 4, weight_steps // 2
    own_mixer.wait()
    mixer_side(0, p).start()
    for k in range(1, half_experts):
        mixer_landed(k)
        mixer_side(k, p).start()
    lax.fori_loop(0, units // 128, down_step, 0)
    total_step(groups - 1)
    returned[pl.ds(pl.multiple_of(e * cap, cap), cap)] = send_stage[0]
    lax.fori_loop(0, first_cut, weight_step, 0)
    for load in late[3:]:
        load.wait()
    first, second = [
        expert_lane == jnp.transpose(jnp.broadcast_to(ids[j : j + 1], (128, tokens)))[:, 0:1]
        for j, expert_lane in enumerate(
            [lax.broadcasted_iota(jnp.int32, (tokens, experts), 1)] * 2
        )
    ]
    expert_lane = lax.broadcasted_iota(jnp.int32, (tokens, experts), 1)
    order = dot((row > col).astype(f32), (first | second).astype(f32)).astype(jnp.int32)
    spots = expert_lane * cap + order
    slot_lane = lax.broadcasted_iota(jnp.int32, (tokens, experts * cap), 1)
    first_slot = jnp.sum(jnp.where(first, spots, 0), axis=1, keepdims=True)
    second_slot = jnp.sum(jnp.where(second, spots, 0), axis=1, keepdims=True)
    pick = ((slot_lane == first_slot) | (slot_lane == second_slot)).astype(f32).astype(bf16)

    def came_back(k, carry):
        source = flip(k)
        spot = returned.at[pl.ds(pl.multiple_of(source * cap, cap), cap)]
        remote(spot, spot, back_send.at[k], back_recv.at[k], (source, p, t)).wait_recv()
        return carry

    lax.fori_loop(1, experts, came_back, 0)
    moe = lax.dot_general(pick, returned[...], PLAIN, preferred_element_type=f32)
    mid_half = (out_grad[:, own_columns].astype(f32) + moe).astype(bf16)
    mid[:, own_columns] = mid_half

    def to_core(columns):
        return remote(mid.at[:, columns], mid.at[:, columns], mid_send, mid_recv, mate_id)

    to_core(own_columns).start()
    share = count // 2
    piece = width // share
    for j in range(share):
        mid_stage[j] = mid_half[:, j * piece : (j + 1) * piece]
    position = position_ref[...]
    q_all = queries[...].astype(f32)
    k_all = keys[...].astype(f32)
    v_all = values[...]
    cumul = [position[:BLK]]
    for n in range(1, blocks):
        cumul.append(position[n * BLK : (n + 1) * BLK] - position[n * BLK - 1 : n * BLK])
    growth = [jnp.exp(c) for c in cumul]
    shrink = [jnp.exp(-c) for c in cumul]
    to_end = [jnp.exp(c[BLK - 1 :] - c) for c in cumul]
    span = [slice(n * BLK, (n + 1) * BLK) for n in range(blocks)]
    q_grow = [(q_all[span[n]] * growth[n]).astype(bf16) for n in range(blocks)]
    k_shrink = [(k_all[span[n]] * shrink[n]).astype(bf16) for n in range(blocks)]
    k_end = [(k_all[span[n]] * to_end[n]).astype(bf16) for n in range(blocks)]
    q_long = (q_all * jnp.exp(position)).astype(bf16)

    to_core(core_columns).wait_recv()
    o_all = dot(mid[...], out_weight[...], ACROSS).astype(bf16)
    for h in range(heads):
        ks, vs = slice(h * DK, (h + 1) * DK), slice(h * DV, (h + 1) * DV)
        summed = dot(q_long[:, ks], o_all[:, vs], DOWNWARD)
        for j in range(per_head):
            sum_stage[h * per_head + j] = summed[j * rows : (j + 1) * rows]
    sum_held[me] = sum_stage[me]
    for k in range(1, count):
        spread(lambda i: sum_stage.at[i], sum_held.at[me], sum_send, sum_recv, k).start()

    direct_half = lax.div(e, half_experts) == t

    def column_copies(act):
        for a in range(half_experts // 2):
            for q in range(2):
                dest_e = t * half_experts + 2 * a + low
                for w in range(2):
                    column = (2 * a + (low if w == 0 else 1 - low)) * 2 + q

                    @pl.when(jnp.logical_or(dest_e != e, q != p))
                    def _():
                        act(
                            remote(
                                mid_stage.at[column], mid_columns.at[w, here],
                                col_send.at[w, a * 2 + q], col_recv.at[w, here], (dest_e, q, t),
                            )
                        )

    column_copies(lambda copy: copy.start())

    @pl.when(direct_half)
    def _():
        base = lax.rem(e, half_experts) - low
        mid_columns[0, here] = mid_stage[(base + low) * 2 + p]
        mid_columns[1, here] = mid_stage[(base + 1 - low) * 2 + p]

    lane_causal = row[:BLK, :BLK] >= col[:BLK, :BLK]
    lane_causal_t = row[:BLK, :BLK] <= col[:BLK, :BLK]
    for n in range(blocks - 1, -1, -1):
        for h in range(heads):
            ks, vs = slice(h * DK, (h + 1) * DK), slice(h * DV, (h + 1) * DV)
            o, v = o_all[span[n], vs], v_all[span[n], vs]
            qg, kk = q_grow[n][:, ks], k_shrink[n][:, ks]
            state_in = block_states[n, h].astype(bf16)
            scores = jnp.where(lane_causal, dot(o, v, ACROSS), 0.0)
            scores_t = jnp.where(lane_causal_t, dot(v, o, ACROSS), 0.0)
            mutual_t = jnp.where(lane_causal_t, dot(kk, qg, ACROSS), 0.0)
            gq = growth[n][:, ks] * (dot(o, state_in, ACROSS) + dot(scores, kk))
            gk = shrink[n][:, ks] * dot(scores_t, qg)
            gv = dot(mutual_t, o)
            if n < blocks - 1:
                later = slice((n + 1) * BLK, tokens)
                end = position[(n + 1) * BLK - 1 : (n + 1) * BLK, ks]
                carried = dot(
                    q_all[later, ks] * jnp.exp(position[later, ks] - end), o_all[later, vs], DOWNWARD
                )
                gk = gk + to_end[n][:, ks] * dot(v, carried, ACROSS)
                gv = gv + dot(k_end[n][:, ks], carried)
            grad_q[span[n], ks] = gq
            key_local[span[n], ks] = gk
            value_local[span[n], vs] = gv
    contrib = q_all * grad_q[...] - k_all * key_local[...]
    contrib_local[...] = contrib
    gathered[me] = jnp.sum(contrib, axis=0, keepdims=True)
    for k in range(1, count):
        spread(lambda i: gathered.at[me], gathered.at[me], term_send, term_recv, k).start()

    lax.fori_loop(first_cut, second_cut, weight_step, 0)
    for k in range(1, count):
        landed(early_held, early_send, early_recv, k)
        landed(sum_held, sum_send, sum_recv, k)
    total = jnp.zeros((rows, DV), f32)
    dots = jnp.zeros((rows, DV), f32)
    for i in range(count - 1, -1, -1):
        result[i] = total
        dot_result[i] = dots
        reach_dot = jnp.sum(early_held[i, 0] * total, axis=1, keepdims=True)
        dots = dots + jnp.broadcast_to(reach_dot, (rows, DV))
        total = early_held[i, 1] * total + sum_held[i]
    from_right[me] = result[me]
    decay_dots[me] = dot_result[me]
    def right_copy(k):
        return spread(lambda i: result.at[i], from_right.at[me], right_send, right_recv, k)

    def dot_copy(k):
        return spread(lambda i: dot_result.at[i], decay_dots.at[me], dot_send, dot_recv, k)

    for k in range(1, count):
        right_copy(k).start()
        dot_copy(k).start()

    def cross_copy():
        return remote(mid_columns, mid_columns, cross_send, cross_recv, mate_id)

    @pl.when(direct_half)
    def _():
        for k in range(1, share):
            source = lax.rem(here + k, share)
            for w in range(2):
                spot = mid_columns.at[w, source]
                remote(
                    spot, spot, col_send.at[w, 0], col_recv.at[w, source], mate_id
                ).wait_recv()
        cross_copy().start()

    lax.fori_loop(second_cut, weight_steps, weight_step, 0)

    @pl.when(jnp.logical_not(direct_half))
    def _():
        cross_copy().wait_recv()

    for k in range(half_experts):
        mixer_side(k, 1 - p).wait_recv()
    for w in (1, 0):
        product = dot(
            mid_columns[w].reshape(share * tokens, piece),
            mixers[...].reshape(share * tokens, mixers.shape[2]),
            DOWNWARD,
        )
        if w:
            near_part[...] = product
            near = remote(near_part, near_held, near_send, near_recv, (flip(1), p, t))
            near.start()
        else:
            grad_out[...] = product
    near.wait_recv()
    grad_out[...] = grad_out[...] + near_held[...]
    for k in range(1, count):
        landed(gathered, term_send, term_recv, k)
    summed_terms = jnp.zeros((1, channels), f32)
    for i in range(count):
        summed_terms += jnp.where(i > me, gathered[i], 0.0)
    right_terms[...] = summed_terms
    for k in range(1, count):
        landed(from_right, right_send, right_recv, k)
        landed(decay_dots, dot_send, dot_recv, k)
    to_core(own_columns).wait_send()
    near.wait_send()
    column_copies(lambda copy: copy.wait_send())

    @pl.when(direct_half)
    def _():
        cross_copy().wait_send()

    for k in range(1, count):
        early_copy(k).wait_send()
        spread(lambda i: sum_stage.at[i], sum_held.at[me], sum_send, sum_recv, k).wait_send()
        right_copy(k).wait_send()
        dot_copy(k).wait_send()
        spread(lambda i: gathered.at[me], gathered.at[me], term_send, term_recv, k).wait_send()

    def close(k, carry):
        for a in range(2):
            to_pair(a, k, p).wait_send()
            to_mate(a, k, p, 0, own_columns).wait_send()
            to_mate(a, k, 1 - p, 1, own_columns).wait_send()
        core_copy(0, k).wait_send()
        core_copy(1, k).wait_send()
        pair_copy(k).wait_send()

        @pl.when(k > 0)
        def _():
            direct(0, k).wait_send()
            direct(1, k).wait_send()
            back_copy(k).wait_send()

        return carry

    lax.fori_loop(0, experts, close, 0)
    for k in range(half_experts):
        if k:
            mixer_copy(k).wait_send()
        mixer_side(k, p).wait_send()
    pltpu.make_async_copy(down_stage, down_out, out_sem.at[0]).wait()
    pltpu.make_async_copy(gate_stage, gate_out, out_sem.at[1]).wait()
    pltpu.make_async_copy(up_stage, up_out, out_sem.at[2]).wait()


def layer_back(
    cap, ids, route_weights, moe_input, out_grad, gate_w, up_w, down_w, mixer, out_weight,
    queries, keys, values, log_decay, block_states,
):
    experts = lax.axis_size("ep")
    count = experts * 2
    tokens, model_width = moe_input.shape
    units = gate_w.shape[1]
    width = model_width // lax.axis_size("tp")
    slots = experts * 2 * cap
    channels = queries.shape[1]
    rows = channels // count
    share = count // 2
    piece = width // share
    half = (experts, cap, width)
    vmem = pl.BlockSpec(memory_space=pltpu.VMEM)
    hbm = pl.BlockSpec(memory_space=pltpu.HBM)
    dma = pltpu.SemaphoreType.DMA
    wide, tall = (model_width, units), (units, model_width)
    kind, f32 = jnp.bfloat16, jnp.float32
    shape = jax.ShapeDtypeStruct
    group_rows = PER_GROUP * 2 * cap
    local = shape((tokens, channels), f32)
    exchanged = shape((count, rows, DV), f32)
    keep = pltpu.VMEM
    return pl.pallas_call(
        functools.partial(experts_kernel, experts, cap),
        out_shape=(
            shape(wide, kind),
            shape(wide, kind),
            shape(tall, kind),
            shape((piece, mixer.shape[1]), f32),
            exchanged,
            exchanged,
            shape((1, channels), f32),
            local,
            local,
            shape(values.shape, f32),
            local,
            local,
            local,
        ),
        in_specs=[vmem] * 4 + [hbm] * 10,
        out_specs=(hbm,) * 3 + (vmem,) * 10,
        scratch_shapes=[
            keep(out_weight.shape, kind),
            keep(queries.shape, kind),
            keep(keys.shape, kind),
            keep(values.shape, kind),
            keep(log_decay.shape, f32),
            keep(block_states.shape, f32),
            keep((share,) + mixer.shape, kind),
            keep((experts * cap, width), kind),
            keep((tokens, channels), f32),
            keep((tokens, model_width), kind),
            keep((share, tokens, piece), kind),
            keep((2, share, tokens, piece), kind),
            keep((count, 2, rows, DV), f32),
            keep((count, 2, rows, DV), f32),
            keep((count, rows, DV), f32),
            keep((count, rows, DV), f32),
            keep((count, rows, DV), f32),
            keep((count, rows, DV), f32),
            keep((count, 1, channels), f32),
            keep((piece, mixer.shape[1]), f32),
            keep((piece, mixer.shape[1]), f32),
            keep((slots, model_width), kind),
            keep((slots, model_width), kind),
            keep((slots, units), kind),
            keep((slots, 2 * units), kind),
            keep((model_width, 2 * units), kind),
            keep(tall, kind),
            keep((group_rows, units), f32),
            keep((group_rows, units), f32),
            keep((slots, model_width), kind),
            keep((experts, tokens), jnp.int32),
            keep(half, kind),
            keep(half, kind),
            keep((2,) + half, kind),
            keep(half, kind),
            keep(half, kind),
            keep(half, kind),
            keep(wide, kind),
            keep(wide, kind),
            keep(tall, kind),
            dma((3,)),
            dma((3,)),
            *(dma((2, experts)) for _ in range(4)),
            *(dma((2, 2, experts)) for _ in range(2)),
            *(dma((2, experts)) for _ in range(2)),
            *(dma((experts,)) for _ in range(4)),
            dma((7,)),
            *(dma((experts // 2,)) for _ in range(4)),
            dma,
            dma,
            dma((2, share)),
            dma((2, share)),
            *(dma for _ in range(4)),
            *(dma((count,)) for _ in range(10)),
        ],
        compiler_params=pltpu.CompilerParams(
            collective_id=0, has_side_effects=True, vmem_limit_bytes=62 * 1024 * 1024
        ),
        name="layer_back",
    )(
        ids, route_weights, moe_input, out_grad, gate_w, up_w, down_w, mixer, out_weight, queries,
        keys, values, log_decay, block_states,
    )


def finish_kernel(
    chunks, grad_out_turned, from_right, decay_dots, right_terms, query_local, key_local,
    value_local, contrib_local, k_fade, fade_out, values, weight_a, weight_b, weight_c,
    grad_q, grad_k, grad_v, grad_decay, grad_out, out_a, out_b, out_c,
    hold_a, hold_b, hold_c, in_sem, out_sem,
):
    f32, bf16 = jnp.float32, jnp.bfloat16
    trios = ((weight_a, hold_a, out_a), (weight_b, hold_b, out_b), (weight_c, hold_c, out_c))

    def moves(a, j):
        source, hold, target = trios[a]
        size = source.shape[0] // chunks
        cut = pl.ds(j * size, size)
        return (
            pltpu.make_async_copy(source.at[cut], hold.at[cut], in_sem.at[a, j]),
            pltpu.make_async_copy(hold.at[cut], target.at[cut], out_sem.at[a, j]),
        )

    steps = [(a, j) for a in range(3) for j in range(chunks)]
    for a, j in steps:
        moves(a, j)[0].start()

    def dot(x, y, dims=(((1,), (0,)), ((), ()))):
        return lax.dot_general(
            x.astype(bf16), y.astype(bf16), dims, preferred_element_type=f32
        )

    def forward(group):
        for a, j in group:
            moves(a, j)[0].wait()
            moves(a, j)[1].start()

    tokens, channels = key_local.shape
    heads = channels // DK
    grad_q[...] = query_local[...].astype(bf16)
    forward(steps[:chunks])
    key_parts = []
    for h in range(heads):
        ks, vs = slice(h * DK, (h + 1) * DK), slice(h * DV, (h + 1) * DV)
        carried = from_right[h].astype(bf16)
        key_parts.append(dot(values[:, vs], carried, ACROSS))
        grad_v[:, vs] = (value_local[:, vs] + dot(k_fade[:, ks], carried)).astype(bf16)
    key_part = jnp.concatenate(key_parts, axis=1)
    grad_k[...] = (key_local[...] + fade_out[...] * key_part).astype(bf16)
    contrib = contrib_local[...] - k_fade[...] * key_part
    forward(steps[chunks : 2 * chunks])
    row = lax.broadcasted_iota(jnp.int32, (tokens, tokens), 0)
    col = lax.broadcasted_iota(jnp.int32, (tokens, tokens), 1)
    later = (col >= row).astype(f32)
    groups = []
    spot = lax.broadcasted_iota(jnp.int32, (128, 128), 0)
    lane = lax.broadcasted_iota(jnp.int32, (128, 128), 1)
    for g in range(channels // 128):
        picked = jnp.where(spot == lane, decay_dots[g * 128 : (g + 1) * 128], 0.0)
        groups.append(jnp.sum(picked, axis=0, keepdims=True))
    right = right_terms[...] - jnp.concatenate(groups, axis=1)
    grad_decay[...] = right + lax.dot_general(
        later, contrib, (((1,), (0,)), ((), ())), precision=PRECISE, preferred_element_type=f32
    )
    grad_out[...] = jnp.transpose(grad_out_turned[...])
    forward(steps[2 * chunks :])
    for a, j in steps:
        moves(a, j)[1].wait()


def finish(local, values, weights):
    grad_out_turned, from_right, decay_dots, right_terms, *rest = local
    tokens, channels = rest[1].shape
    heads = channels // DK
    from_right = from_right.reshape(heads, DK, DV)
    decay_dots = decay_dots.reshape(channels, DV)
    vmem = pl.BlockSpec(memory_space=pltpu.VMEM)
    hbm = pl.BlockSpec(memory_space=pltpu.HBM)
    dma = pltpu.SemaphoreType.DMA
    shape = jax.ShapeDtypeStruct
    f32, bf16 = jnp.float32, jnp.bfloat16
    chunks = 4
    return pl.pallas_call(
        functools.partial(finish_kernel, chunks),
        out_shape=(
            shape((tokens, channels), bf16),
            shape((tokens, channels), bf16),
            shape((tokens, heads * DV), bf16),
            shape((tokens, channels), f32),
            shape(grad_out_turned.shape[::-1], f32),
            *(shape(w.shape, w.dtype) for w in weights),
        ),
        in_specs=[vmem] * 11 + [hbm] * 3,
        out_specs=(vmem,) * 5 + (hbm,) * 3,
        scratch_shapes=[pltpu.VMEM(w.shape, w.dtype) for w in weights]
        + [dma((3, chunks)), dma((3, chunks))],
        compiler_params=pltpu.CompilerParams(vmem_limit_bytes=60 * 1024 * 1024),
        name="finish",
    )(grad_out_turned, from_right, decay_dots, right_terms, *rest, values, *weights)


def body(
    moe_input,
    out_grad,
    route_ids,
    route_weights,
    gate_w,
    up_w,
    down_w,
    mixer_out,
    out_weight,
    queries,
    keys,
    values,
    log_decay,
    block_states,
):
    experts = lax.axis_size("ep")
    cap = -(-3 * moe_input.shape[0] // experts // 16) * 16
    results = layer_back(
        cap, route_ids.T, route_weights.T, moe_input, out_grad, gate_w[0], up_w[0], down_w[0],
        mixer_out, out_weight, queries, keys, values, log_decay, block_states,
    )
    weights, local = results[:3], results[3:]
    grad_q, grad_k, grad_v, grad_decay, grad_out_weight, grad_gate, grad_up, grad_down = finish(
        local, values, weights
    )
    return (
        grad_q,
        grad_k,
        grad_v,
        grad_decay,
        grad_out_weight,
        grad_gate[None],
        grad_up[None],
        grad_down[None],
    )


def solution(mesh):
    sp_count, tp_count = mesh.devices.shape
    mesh = Mesh(mesh.devices.reshape(sp_count // 2, 2, tp_count), ("ep", "pair", "tp"))
    placed = (
        P(SP, None),
        P(SP, None),
        P(SP, None),
        P(SP, None),
        P(SP, None, "tp"),
        P(SP, None, "tp"),
        P(SP, "tp", None),
        P(SP, "tp"),
        P("tp", None),
        P(SP, "tp"),
        P(SP, "tp"),
        P(SP, "tp"),
        P(SP, "tp"),
        P(SP, "tp", None, None),
    )
    return jax.shard_map(
        body,
        mesh=mesh,
        in_specs=placed,
        out_specs=(
            P(SP, "tp"),
            P(SP, "tp"),
            P(SP, "tp"),
            P(SP, "tp"),
            P("tp", SP),
            P(SP, None, "tp"),
            P(SP, None, "tp"),
            P(SP, "tp", None),
        ),
        check_vma=False,
    )
```

time: 170 us -> 135 us (0.79)
  Pallas kernels: 155 us -> 132 us
  between operations: 14.1 us -> 0.81 us
    pallas_call x2 -> x1, Pallas kernels: 144 us -> 121 us  [layer_back(): pl.pallas_call(functools.partial(experts_kernel, experts, cap), out_shape...]
  transfers between devices with their start and end apart: 1 -> 0, of which waited for: 0 -> 0; matrix products, arithmetic and copies ran while one was open for 0% -> 0% of each run, Pallas kernels for 85% -> 0%
where the time goes in v2:
time: 135 us; the launch traced here: 133 us
  Pallas kernels  132 us (98%)
    pallas_call x1, Pallas kernels, layer_back(): pl.pallas_call(functools.partial(experts_kernel, experts, cap), out_shape...  121 us
    pallas_call x1, Pallas kernels, finish(): pl.pallas_call(functools.partial(finish_kernel, chunks), out_shape=(shape...  10.9 us

profile of v2, /device:TPU:0, one launch (start us, length us, event | category | flops | bytes accessed | tf_op | source)
XLA Modules:
  0.0 132.8 jit_solution(11052160775721307941)
XLA Ops:
  0.6 121.2 %layer_back.1 = (bf16[2048,896]{1,0:T(8,128)(2,1)}, bf16[2048,896]{1,0:T(8,128)(2,1)}, bf16[896,2048]{1,0:T(8,128)(2,1)}, f32[128,512]{1,0:T(8,128)}, f32[16,16,...) custom-call(s32[2,128]{1,0:T(2,128)} %bitcast.15, ...), custom_call_target="tpu_custom_call" | custom-call | tf_op jit(solution)/shard_map/layer_back/pallas_call | solution.py:647
  121.8 10.9 %finish.1 = (bf16[128,256]{1,0:T(8,128)(2,1)}, bf16[128,256]{1,0:T(8,128)(2,1)}, bf16[128,512]{1,0:T(8,128)(2,1)}, f32[128,256]{1,0:T(8,128)}, f32[512,128]{1,0:...) custom-call(f32[128,512]{1,0:T(8,128)} %get-tuple-element.29.grad_out_turned, ...), custom_call_target="tpu_custom_call" | custom-call | tf_op jit(solution)/shard_map/finish/pallas_call | solution.py:809

commit v3 on v2

--- a/solution.py
+++ b/solution.py
@@ -37,14 +37,14 @@
     value_local, contrib_local, k_fade, fade_out,
     out_weight, queries, keys, values, log_decay, block_states, mixers, returned, position_ref,
     mid, mid_stage, mid_columns, early_stage, early_held, sum_stage, sum_held, result, dot_result,
-    gathered, near_part, near_held,
+    gathered, gains, near_part, near_held,
     toks, grads, hidden, d_both, gate_up, down, silu_part, slope_part, parts, rank, tok_send,
-    grad_send, core_held, pair_stage, pair_held, send_stage, gate_stage, up_stage, down_stage,
-    weight_sem, out_sem, direct_send, direct_recv, pass_send, pass_recv, mate_send, mate_recv,
+    grad_send, core_held, pair_held,
+    weight_sem, direct_send, direct_recv, pass_send, pass_recv, mate_send, mate_recv,
     core_send, core_recv, pair_send, pair_recv, back_send, back_recv,
     load_sem, mixer_send, mixer_recv, side_send, side_recv, mid_send, mid_recv, col_send, col_recv,
     cross_send, cross_recv, near_send, near_recv, early_send, early_recv, sum_send, sum_recv,
-    right_send, right_recv, dot_send, dot_recv, term_send, term_recv,
+    right_send, right_recv, dot_send, dot_recv, term_send, term_recv, gain_send, gain_recv,
 ):
     e, p, t = lax.axis_index("ep"), lax.axis_index("pair"), lax.axis_index("tp")
     f32, bf16 = jnp.float32, jnp.bfloat16
@@ -220,16 +220,20 @@
     faded = keys[...].astype(f32) * fade
     fade_out[...] = fade
     k_fade[...] = faded
-    gain = jnp.transpose(jnp.broadcast_to(jnp.exp(device_total), (DV, channels)))
+    gains[me] = jnp.exp(device_total)
     for h in range(heads):
         ks, vs = slice(h * DK, (h + 1) * DK), slice(h * DV, (h + 1) * DV)
         reach = dot(faded[:, ks], values[:, vs], DOWNWARD)
         for j in range(per_head):
-            early_stage[h * per_head + j, 0] = reach[j * rows : (j + 1) * rows]
-            early_stage[h * per_head + j, 1] = gain[h * DK + j * rows : h * DK + (j + 1) * rows]
+            early_stage[h * per_head + j] = reach[j * rows : (j + 1) * rows].astype(bf16)
     early_held[me] = early_stage[me]
+
+    def gain_copy(k):
+        return spread(lambda i: gains.at[me], gains.at[me], gain_send, gain_recv, k)
+
     for k in range(1, count):
         early_copy(k).start()
+        gain_copy(k).start()
     for load in loads:
         load.wait()
 
@@ -257,12 +261,12 @@
 
     def pair_copy(k):
         return remote(
-            pair_stage.at[k], pair_held.at[k], pair_send.at[k], pair_recv.at[k], pair_id
+            parts.at[block(k, 1 - p), own_columns], pair_held.at[k], pair_send.at[k], pair_recv.at[k], pair_id
         )
 
     def back_copy(k):
         return remote(
-            send_stage.at[k], returned.at[pl.ds(pl.multiple_of(e * cap, cap), cap)], back_send.at[k], back_recv.at[k], (flip(k), p, t)
+            parts.at[block(k, p), own_columns], returned.at[pl.ds(pl.multiple_of(e * cap, cap), cap)], back_send.at[k], back_recv.at[k], (flip(k), p, t)
         )
 
     def half_of(which, k):
@@ -276,7 +280,7 @@
     def half_step(g):
         for k in members(g):
             core_copy(0, k).wait_recv()
-            pair_stage[k] = half_of(0, k)
+            parts[block(k, 1 - p), own_columns] = half_of(0, k)
             pair_copy(k).start()
 
     def total_step(g):
@@ -284,7 +288,7 @@
             core_copy(1, k).wait_recv()
             pair_copy(k).wait_recv()
             total = half_of(1, k).astype(f32) + pair_held[k].astype(f32)
-            send_stage[k] = total.astype(bf16)
+            parts[block(k, p), own_columns] = total.astype(bf16)
 
             @pl.when(k > 0)
             def _():
@@ -361,10 +365,9 @@
 
     def down_step(i, carry):
         cut = pl.ds(pl.multiple_of(i * 128, 128), 128)
-        down_stage[cut, :] = lax.dot_general(
+        down_out[cut, :] = lax.dot_general(
             hidden[:, cut], grads[...], DOWNWARD, preferred_element_type=f32
         ).astype(bf16)
-        pltpu.make_async_copy(down_stage.at[cut], down_out.at[cut], out_sem.at[0]).start()
         return carry
 
     def weight_step(i, carry):
@@ -372,10 +375,8 @@
         both = lax.dot_general(
             toks[:, cut], d_both[...], DOWNWARD, preferred_element_type=f32
         ).astype(bf16)
-        gate_stage[cut, :] = both[:, :units]
-        up_stage[cut, :] = both[:, units:]
-        pltpu.make_async_copy(gate_stage.at[cut], gate_out.at[cut], out_sem.at[1]).start()
-        pltpu.make_async_copy(up_stage.at[cut], up_out.at[cut], out_sem.at[2]).start()
+        gate_out[cut, :] = both[:, :units]
+        up_out[cut, :] = both[:, units:]
         return carry
 
     weight_steps = model_width // 256
@@ -387,7 +388,9 @@
         mixer_side(k, p).start()
     lax.fori_loop(0, units // 128, down_step, 0)
     total_step(groups - 1)
-    returned[pl.ds(pl.multiple_of(e * cap, cap), cap)] = send_stage[0]
+    returned[pl.ds(pl.multiple_of(e * cap, cap), cap)] = parts[
+        block(0, p), own_columns
+    ]
     lax.fori_loop(0, first_cut, weight_step, 0)
     for load in late[3:]:
         load.wait()
@@ -446,7 +449,7 @@
         ks, vs = slice(h * DK, (h + 1) * DK), slice(h * DV, (h + 1) * DV)
         summed = dot(q_long[:, ks], o_all[:, vs], DOWNWARD)
         for j in range(per_head):
-            sum_stage[h * per_head + j] = summed[j * rows : (j + 1) * rows]
+            sum_stage[h * per_head + j] = summed[j * rows : (j + 1) * rows].astype(bf16)
     sum_held[me] = sum_stage[me]
     for k in range(1, count):
         spread(lambda i: sum_stage.at[i], sum_held.at[me], sum_send, sum_recv, k).start()
@@ -512,14 +515,26 @@
     for k in range(1, count):
         landed(early_held, early_send, early_recv, k)
         landed(sum_held, sum_send, sum_recv, k)
+        landed(gains, gain_send, gain_recv, k)
     total = jnp.zeros((rows, DV), f32)
-    dots = jnp.zeros((rows, DV), f32)
+    dots = jnp.zeros((rows, 1), f32)
+    table = jnp.zeros((rows, 128), f32)
+    table_lane = lax.broadcasted_iota(jnp.int32, (rows, 128), 1)
+    table_row = lax.broadcasted_iota(jnp.int32, (rows, 128), 0)
+    channel = lax.broadcasted_iota(jnp.int32, (rows, channels), 1)
+    owned = channel == me * rows + lax.broadcasted_iota(jnp.int32, (rows, channels), 0)
     for i in range(count - 1, -1, -1):
-        result[i] = total
-        dot_result[i] = dots
-        reach_dot = jnp.sum(early_held[i, 0] * total, axis=1, keepdims=True)
-        dots = dots + jnp.broadcast_to(reach_dot, (rows, DV))
-        total = early_held[i, 1] * total + sum_held[i]
+        result[i] = total.astype(bf16)
+        table = jnp.where(table_lane == i, dots, table)
+        dots = dots + jnp.sum(early_held[i].astype(f32) * total, axis=1, keepdims=True)
+        gain = jnp.sum(jnp.where(owned, gains[i], 0.0), axis=1, keepdims=True)
+        total = gain * total + sum_held[i].astype(f32)
+    spread_out = (table_lane == lax.rem(me * rows, 128) + table_row).astype(f32)
+    turned = lax.dot_general(
+        table, spread_out, DOWNWARD, precision=PRECISE, preferred_element_type=f32
+    )
+    for i in range(count):
+        dot_result[i] = turned[i : i + 1]
     from_right[me] = result[me]
     decay_dots[me] = dot_result[me]
     def right_copy(k):
@@ -587,6 +602,7 @@
 
     for k in range(1, count):
         early_copy(k).wait_send()
+        gain_copy(k).wait_send()
         spread(lambda i: sum_stage.at[i], sum_held.at[me], sum_send, sum_recv, k).wait_send()
         right_copy(k).wait_send()
         dot_copy(k).wait_send()
@@ -614,9 +630,6 @@
         if k:
             mixer_copy(k).wait_send()
         mixer_side(k, p).wait_send()
-    pltpu.make_async_copy(down_stage, down_out, out_sem.at[0]).wait()
-    pltpu.make_async_copy(gate_stage, gate_out, out_sem.at[1]).wait()
-    pltpu.make_async_copy(up_stage, up_out, out_sem.at[2]).wait()
 
 
 def layer_back(
@@ -642,8 +655,8 @@
     shape = jax.ShapeDtypeStruct
     group_rows = PER_GROUP * 2 * cap
     local = shape((tokens, channels), f32)
-    exchanged = shape((count, rows, DV), f32)
     keep = pltpu.VMEM
+    grant = 40 if slots * model_width <= 3 << 19 else 60
     return pl.pallas_call(
         functools.partial(experts_kernel, experts, cap),
         out_shape=(
@@ -651,8 +664,8 @@
             shape(wide, kind),
             shape(tall, kind),
             shape((piece, mixer.shape[1]), f32),
-            exchanged,
-            exchanged,
+            shape((count, rows, DV), kind),
+            shape((count, 1, 128), f32),
             shape((1, channels), f32),
             local,
             local,
@@ -662,7 +675,7 @@
             local,
         ),
         in_specs=[vmem] * 4 + [hbm] * 10,
-        out_specs=(hbm,) * 3 + (vmem,) * 10,
+        out_specs=(vmem,) * 13,
         scratch_shapes=[
             keep(out_weight.shape, kind),
             keep(queries.shape, kind),
@@ -676,12 +689,13 @@
             keep((tokens, model_width), kind),
             keep((share, tokens, piece), kind),
             keep((2, share, tokens, piece), kind),
-            keep((count, 2, rows, DV), f32),
-            keep((count, 2, rows, DV), f32),
-            keep((count, rows, DV), f32),
-            keep((count, rows, DV), f32),
-            keep((count, rows, DV), f32),
-            keep((count, rows, DV), f32),
+            keep((count, rows, DV), kind),
+            keep((count, rows, DV), kind),
+            keep((count, rows, DV), kind),
+            keep((count, rows, DV), kind),
+            keep((count, rows, DV), kind),
+            keep((count, 1, 128), f32),
+            keep((count, 1, channels), f32),
             keep((count, 1, channels), f32),
             keep((piece, mixer.shape[1]), f32),
             keep((piece, mixer.shape[1]), f32),
@@ -699,12 +713,6 @@
             keep(half, kind),
             keep((2,) + half, kind),
             keep(half, kind),
-            keep(half, kind),
-            keep(half, kind),
-            keep(wide, kind),
-            keep(wide, kind),
-            keep(tall, kind),
-            dma((3,)),
             dma((3,)),
             *(dma((2, experts)) for _ in range(4)),
             *(dma((2, 2, experts)) for _ in range(2)),
@@ -717,81 +725,87 @@
             dma((2, share)),
             dma((2, share)),
             *(dma for _ in range(4)),
-            *(dma((count,)) for _ in range(10)),
+            *(dma((count,)) for _ in range(12)),
         ],
         compiler_params=pltpu.CompilerParams(
-            collective_id=0, has_side_effects=True, vmem_limit_bytes=62 * 1024 * 1024
+            collective_id=0, has_side_effects=True, vmem_limit_bytes=grant * 1024 * 1024
         ),
         name="layer_back",
     )(
-        ids, route_weights, moe_input, out_grad, gate_w, up_w, down_w, mixer, out_weight, queries,
-        keys, values, log_decay, block_states,
+        *(
+            pltpu.with_memory_space_constraint(x, pltpu.HBM)
+            for x in (
+                ids, route_weights, moe_input, out_grad, gate_w, up_w, down_w, mixer, out_weight,
+                queries, keys, values, log_decay, block_states,
+            )
+        )
     )
 
 
 def finish_kernel(
-    chunks, grad_out_turned, from_right, decay_dots, right_terms, query_local, key_local,
-    value_local, contrib_local, k_fade, fade_out, values, weight_a, weight_b, weight_c,
-    grad_q, grad_k, grad_v, grad_decay, grad_out, out_a, out_b, out_c,
-    hold_a, hold_b, hold_c, in_sem, out_sem,
+    chunks, weight_a, weight_b, weight_c, *refs,
 ):
     f32, bf16 = jnp.float32, jnp.bfloat16
-    trios = ((weight_a, hold_a, out_a), (weight_b, hold_b, out_b), (weight_c, hold_c, out_c))
-
-    def moves(a, j):
-        source, hold, target = trios[a]
+    sources, targets, holds = refs[:11], refs[11:19], refs[19:30]
+    small_sem, out_sem = refs[30:]
+    grad_q, grad_k, grad_v, grad_decay, grad_out, out_a, out_b, out_c = targets
+    pairs = ((weight_a, out_a), (weight_b, out_b), (weight_c, out_c))
+    small = [
+        pltpu.make_async_copy(src, dst, small_sem.at[i])
+        for i, (src, dst) in enumerate(zip(sources, holds))
+    ]
+
+    def move(a, j):
+        source, target = pairs[a]
         size = source.shape[0] // chunks
         cut = pl.ds(j * size, size)
-        return (
-            pltpu.make_async_copy(source.at[cut], hold.at[cut], in_sem.at[a, j]),
-            pltpu.make_async_copy(hold.at[cut], target.at[cut], out_sem.at[a, j]),
-        )
+        return pltpu.make_async_copy(source.at[cut], target.at[cut], out_sem.at[a, j])
 
     steps = [(a, j) for a in range(3) for j in range(chunks)]
+    for copy in small:
+        copy.start()
     for a, j in steps:
-        moves(a, j)[0].start()
-
-    def dot(x, y, dims=(((1,), (0,)), ((), ()))):
+        move(a, j).start()
+
+    def dot(x, y, dims=PLAIN):
         return lax.dot_general(
             x.astype(bf16), y.astype(bf16), dims, preferred_element_type=f32
         )
 
-    def forward(group):
-        for a, j in group:
-            moves(a, j)[0].wait()
-            moves(a, j)[1].start()
-
+    for copy in small:
+        copy.wait()
+    (
+        grad_out_turned, from_right, decay_dots, right_terms, query_local, key_local, value_local,
+        contrib_local, k_fade, fade_out, values,
+    ) = holds
     tokens, channels = key_local.shape
     heads = channels // DK
     grad_q[...] = query_local[...].astype(bf16)
-    forward(steps[:chunks])
     key_parts = []
     for h in range(heads):
         ks, vs = slice(h * DK, (h + 1) * DK), slice(h * DV, (h + 1) * DV)
-        carried = from_right[h].astype(bf16)
+        carried = from_right[h]
         key_parts.append(dot(values[:, vs], carried, ACROSS))
         grad_v[:, vs] = (value_local[:, vs] + dot(k_fade[:, ks], carried)).astype(bf16)
     key_part = jnp.concatenate(key_parts, axis=1)
     grad_k[...] = (key_local[...] + fade_out[...] * key_part).astype(bf16)
     contrib = contrib_local[...] - k_fade[...] * key_part
-    forward(steps[chunks : 2 * chunks])
     row = lax.broadcasted_iota(jnp.int32, (tokens, tokens), 0)
     col = lax.broadcasted_iota(jnp.int32, (tokens, tokens), 1)
     later = (col >= row).astype(f32)
-    groups = []
-    spot = lax.broadcasted_iota(jnp.int32, (128, 128), 0)
-    lane = lax.broadcasted_iota(jnp.int32, (128, 128), 1)
-    for g in range(channels // 128):
-        picked = jnp.where(spot == lane, decay_dots[g * 128 : (g + 1) * 128], 0.0)
-        groups.append(jnp.sum(picked, axis=0, keepdims=True))
+    owners = decay_dots.shape[0]
+    each = owners * 128 // channels
+    groups = [
+        jnp.sum(decay_dots[g * each : (g + 1) * each, 0], axis=0, keepdims=True)
+        for g in range(channels // 128)
+    ]
     right = right_terms[...] - jnp.concatenate(groups, axis=1)
     grad_decay[...] = right + lax.dot_general(
-        later, contrib, (((1,), (0,)), ((), ())), precision=PRECISE, preferred_element_type=f32
+        later, contrib, PLAIN, precision=PRECISE, preferred_element_type=f32
     )
     grad_out[...] = jnp.transpose(grad_out_turned[...])
-    forward(steps[2 * chunks :])
     for a, j in steps:
-        moves(a, j)[1].wait()
+        move(a, j).wait()
 
 
 def finish(local, values, weights):
@@ -799,13 +813,15 @@
     tokens, channels = rest[1].shape
     heads = channels // DK
     from_right = from_right.reshape(heads, DK, DV)
-    decay_dots = decay_dots.reshape(channels, DV)
     vmem = pl.BlockSpec(memory_space=pltpu.VMEM)
     hbm = pl.BlockSpec(memory_space=pltpu.HBM)
     dma = pltpu.SemaphoreType.DMA
     shape = jax.ShapeDtypeStruct
     f32, bf16 = jnp.float32, jnp.bfloat16
-    chunks = 4
+    chunks = 8
+    smalls = (
+        grad_out_turned, from_right, decay_dots, right_terms, *rest, values,
+    )
     return pl.pallas_call(
         functools.partial(finish_kernel, chunks),
         out_shape=(
@@ -816,13 +832,13 @@
             shape(grad_out_turned.shape[::-1], f32),
             *(shape(w.shape, w.dtype) for w in weights),
         ),
-        in_specs=[vmem] * 11 + [hbm] * 3,
+        in_specs=[vmem] * 3 + [hbm] * 11,
         out_specs=(vmem,) * 5 + (hbm,) * 3,
-        scratch_shapes=[pltpu.VMEM(w.shape, w.dtype) for w in weights]
-        + [dma((3, chunks)), dma((3, chunks))],
-        compiler_params=pltpu.CompilerParams(vmem_limit_bytes=60 * 1024 * 1024),
+        scratch_shapes=[pltpu.VMEM(w.shape, w.dtype) for w in smalls]
+        + [dma((11,)), dma((3, chunks))],
+        compiler_params=pltpu.CompilerParams(vmem_limit_bytes=8 * 1024 * 1024),
         name="finish",
-    )(grad_out_turned, from_right, decay_dots, right_terms, *rest, values, *weights)
+    )(*weights, *smalls)
 
 
 def body(

time: 135 us -> 124 us (0.919); the launches traced: 133 us -> 124 us
  Pallas kernels: 132 us -> 123 us
    pallas_call x1, Pallas kernels: 10.9 us -> 6.38 us  [finish(): pl.pallas_call(functools.partial(finish_kernel, chunks), out_shape=(shape...]
    pallas_call x1, Pallas kernels: 121 us -> 117 us  [layer_back(): pl.pallas_call(functools.partial(experts_kernel, experts, cap), out_shape...]
where the time goes in v3:
time: 124 us
  Pallas kernels  123 us (99%)
    pallas_call x1, Pallas kernels, layer_back(): pl.pallas_call(functools.partial(experts_kernel, experts, cap), out_shape...  117 us
    pallas_call x1, Pallas kernels, finish(): pl.pallas_call(functools.partial(finish_kernel, chunks), out_shape=(shape...  6.38 us

profile of v3, /device:TPU:0, one launch (start us, length us, event | category | flops | bytes accessed | tf_op | source)
XLA Modules:
  0.0 123.9 jit_solution(9324576783292338829)
XLA Ops:
  0.6 0.0 copy-start
  0.6 116.7 %layer_back.1 = (bf16[2048,896]{1,0:T(8,128)(2,1)S(1)}, bf16[2048,896]{1,0:T(8,128)(2,1)S(1)}, bf16[896,2048]{1,0:T(8,128)(2,1)S(1)}, f32[128,512]{1,0:T(8,128)S...) custom-call(s32[2,128]{1,0:T(2,128)} %bitcast.13, ...), custom_call_target="tpu_custom_call" | custom-call | tf_op jit(solution)/shard_map/layer_back/pallas_call | solution.py:660
  117.3 0.0 copy-done
  117.3 6.4 %finish.1 = (bf16[128,256]{1,0:T(8,128)(2,1)}, bf16[128,256]{1,0:T(8,128)(2,1)}, bf16[128,512]{1,0:T(8,128)(2,1)}, f32[128,256]{1,0:T(8,128)}, f32[512,128]{1,0:...) custom-call(bf16[2048,896]{1,0:T(8,128)(2,1)S(1)} %get-tuple-element.29.weight_a, ...), custom_call_target="tpu_custom_call" | custom-call | tf_op jit(solution)/shard_map/finish/pallas_call | solution.py:825
Async XLA Ops:
  0.6 116.7 %copy-start = (bf16[128,512]{1,0:T(8,128)(2,1)S(1)}, bf16[128,512]{1,0:T(8,128)(2,1)}, u32[]{:S(2)}) copy-start(bf16[128,512]{1,0:T(8,128)(2,1)} %refs_10_.1) | copy-start | bytes 393220
